TPU v7x, 32 devices: a whole 2x2x4 slice. The times are simulated.
32 devices in a mesh: ep: 8 (over z, core), tp: 4 (over y, x).
Axes of the slice: x: 2, y: 2, z: 4, core: 2. Of those that a mesh axis runs over, the one named last changes fastest.
Arguments:
- tokens: bfloat16 [384, 2048], P('ep'), may hold values from -6 to 6
- retention_state: float32 [384, 16, 64, 64], P('ep', 'tp'), may hold values from -1.5 to 1.5
- lengths: int32 [384], P('ep'), may hold values from 1024 to 16383
- query_weight: bfloat16 [2048, 1024], P(None, 'tp'), may hold values from -0.125 to 0.125
- key_weight: bfloat16 [2048, 1024], P(None, 'tp'), may hold values from -0.125 to 0.125
- value_weight: bfloat16 [2048, 1024], P(None, 'tp'), may hold values from -0.125 to 0.125
- gate_weight: bfloat16 [2048, 1024], P(None, 'tp'), may hold values from -0.125 to 0.125
- out_weight: bfloat16 [1024, 2048], P(None, 'tp'), may hold values from -0.1875 to 0.1875
- first_gain: float32 [2048], replicated, may hold values from 0.1 to 1.9
- routing: int32 [384, 4], P('ep'), may hold values from 0 to 31, all different within a row; in each aligned block of 48 rows (0 to 47, 48 to 95, ...) at most 18 rows name the same one
- route_weight: float32 [384, 4], P('ep'), may hold values from 0.1 to 1
- expert_gate: bfloat16 [32, 2048, 512], P('ep', None, 'tp'), may hold values from -0.125 to 0.125
- expert_up: bfloat16 [32, 2048, 512], P('ep', None, 'tp'), may hold values from -0.125 to 0.125
- expert_down: bfloat16 [32, 512, 2048], P('ep', None, 'tp'), may hold values from -0.25 to 0.25
- shared_gate: bfloat16 [2048, 512], P(None, 'tp'), may hold values from -0.125 to 0.125
- shared_up: bfloat16 [2048, 512], P(None, 'tp'), may hold values from -0.125 to 0.125
- shared_down: bfloat16 [512, 2048], P(None, 'tp'), may hold values from -0.25 to 0.25
- side_gate: bfloat16 [2048, 256], P('ep', 'tp'), may hold values from -0.125 to 0.125
- side_up: bfloat16 [2048, 256], P('ep', 'tp'), may hold values from -0.125 to 0.125
- side_down: bfloat16 [256, 2048], P(None, 'tp'), may hold values from -0.375 to 0.375
- side_switch: bfloat16 [2048], replicated, may hold values from -0.125 to 0.125
- second_gain: float32 [2048], P('tp'), may hold values from 0.1 to 1.9
Outputs:
- output: bfloat16 [384, 2048], P('ep', 'tp')
- new_state: float32 [384, 16, 64, 64], P('ep', 'tp')
Inputs may be any that keep to these rules, and one draw needn't show every extreme that they name: `routing`: each row names 4 different experts. Among the rows of one ep index (aligned blocks of 48 rows) no expert is named by more than 18 rows, a bound that some block reaches.
All inputs are finite; a program needn't handle non-finite values.
Results may differ from a plain program's by a relative error of at most 0.013.
Values may be sent and summed in bfloat16 or wider, within the bound.
A program may use at most 64 MiB of HBM per device.

v0:
```python
import functools

import jax
import jax.numpy as jnp
from jax import lax
from jax.experimental import pallas as pl
from jax.experimental.pallas import tpu as pltpu
from jax.sharding import PartitionSpec as P

HEADS = 16


RESIDUAL_SCALE = 2.0**0.25
NORM_EPS = 1e-05
GROUP_EPS = 1e-06
ROPE_BASE = 10000.0


def rotate(vector, positions):
    half_width = vector.shape[-1] // 2
    frequency = ROPE_BASE ** (-jnp.arange(half_width, dtype=jnp.float32) / half_width)
    angles = positions.astype(jnp.float32)[:, None, None] * frequency[None, None, :]
    cosine = jnp.cos(angles)
    sine_part = jnp.sin(angles)
    first_half = vector[..., :half_width]
    second_half = vector[..., half_width:]
    return jnp.concatenate(
        [
            first_half * cosine - second_half * sine_part,
            second_half * cosine + first_half * sine_part,
        ],
        -1,
    )


def retain(
    retention_state,
    lengths,
    projections,
    first_head,
):
    row_count = retention_state.shape[0]
    head_count = retention_state.shape[1]
    head_width = retention_state.shape[2]

    query_rows, key_part, value_part, gate_part = [part.astype(jnp.float32) for part in projections]
    queries = rotate(query_rows.reshape(row_count, head_count, head_width), lengths)
    key_rows = rotate(
        key_part.reshape(row_count, head_count, head_width), lengths
    ) * head_width ** (-0.5)
    values = value_part.reshape(row_count, head_count, head_width)
    gate_act = gate_part
    head_index = (first_head + jnp.arange(head_count)).astype(jnp.float32)
    decays = 1.0 - 2.0 ** (-5.0 - 7.0 * head_index / (HEADS - 1))
    own_term = jnp.sum(queries * key_rows, -1, keepdims=True) * values
    carried = decays[None, :, None] * jnp.sum(queries[:, :, :, None] * retention_state, 2)
    result = own_term + carried
    new_state = (
        decays[None, :, None, None] * retention_state
        + key_rows[:, :, :, None] * values[:, :, None, :]
    )
    normed = result * lax.rsqrt(jnp.mean(result * result, -1, keepdims=True) + GROUP_EPS)
    mixed_heads = (
        normed.reshape(row_count, head_count * head_width) * jax.nn.silu(gate_act)
    ).astype(jnp.bfloat16)
    return (mixed_heads, new_state)


VMEM = pl.BlockSpec(memory_space=pltpu.VMEM)
DEVICE = pl.DeviceIdType.MESH


def enter(peers):
    barrier = pltpu.get_barrier_semaphore()
    for peer in peers:
        pl.semaphore_signal(barrier, inc=1, device_id=peer, device_id_type=DEVICE)
    pl.semaphore_wait(barrier, len(peers))


def send(source, target, send_sem, recv_sem, peer):
    copy = pltpu.make_async_remote_copy(
        src_ref=source,
        dst_ref=target,
        send_sem=send_sem,
        recv_sem=recv_sem,
        device_id=peer,
        device_id_type=DEVICE,
    )
    copy.start()
    return copy


def on_axis(axis, index):
    if axis == "ep":
        return (index, lax.axis_index("tp"))
    return (lax.axis_index("ep"), index)


def gather_body(axis, count, parts, *refs):
    sources, targets = refs[:parts], refs[parts : 2 * parts]
    send_sem, recv_sem, local_sem = refs[2 * parts :]
    me = lax.axis_index(axis)
    others = [lax.rem(me + step, count) for step in range(1, count)]
    locals_ = []
    for part in range(parts):
        own = pltpu.make_async_copy(sources[part], targets[part].at[me], local_sem.at[part])
        own.start()
        locals_.append(own)
    enter([on_axis(axis, other) for other in others])
    copies = []
    for step, other in enumerate(others):
        for part in range(parts):
            copies.append(
                send(
                    sources[part],
                    targets[part].at[me],
                    send_sem.at[step, part],
                    recv_sem.at[step, part],
                    on_axis(axis, other),
                )
            )
    for copy in locals_:
        copy.wait()
    for copy in copies:
        copy.wait()


def gather(arrays, axis, ident):
    count, parts = lax.axis_size(axis), len(arrays)
    return pl.pallas_call(
        functools.partial(gather_body, axis, count, parts),
        out_shape=[jax.ShapeDtypeStruct((count,) + a.shape, a.dtype) for a in arrays],
        in_specs=[VMEM] * parts,
        out_specs=[VMEM] * parts,
        scratch_shapes=[
            pltpu.SemaphoreType.DMA((count - 1, parts)),
            pltpu.SemaphoreType.DMA((count - 1, parts)),
            pltpu.SemaphoreType.DMA((parts,)),
        ],
        compiler_params=pltpu.CompilerParams(collective_id=ident, has_side_effects=True),
    )(*arrays)


def scatter_body(count, source, target, send_sem, recv_sem, local_sem):
    me = lax.axis_index("ep")
    others = [lax.rem(me + step, count) for step in range(1, count)]
    own = pltpu.make_async_copy(source.at[me], target.at[me], local_sem)
    own.start()
    enter([on_axis("ep", other) for other in others])
    copies = [
        send(
            source.at[other],
            target.at[me],
            send_sem.at[step],
            recv_sem.at[step],
            on_axis("ep", other),
        )
        for step, other in enumerate(others)
    ]
    own.wait()
    for copy in copies:
        copy.wait()


def scatter(array, ident):
    count = array.shape[0]
    return pl.pallas_call(
        functools.partial(scatter_body, count),
        out_shape=jax.ShapeDtypeStruct(array.shape, array.dtype),
        in_specs=[VMEM],
        out_specs=VMEM,
        scratch_shapes=[
            pltpu.SemaphoreType.DMA((count - 1,)),
            pltpu.SemaphoreType.DMA((count - 1,)),
            pltpu.SemaphoreType.DMA,
        ],
        compiler_params=pltpu.CompilerParams(collective_id=ident, has_side_effects=True),
    )(array)


def first_body(count, *refs):
    parts = 3
    sources, (tokens, *weights) = refs[:parts], refs[parts : parts + 5]
    targets = refs[parts + 5 : 2 * parts + 5]
    results = refs[2 * parts + 5 : 2 * parts + 9]
    send_sem, recv_sem, local_sem = refs[2 * parts + 9 :]
    chips = count // 2
    me = lax.axis_index("ep")
    chip, core = me // 2, lax.rem(me, 2)
    partner = on_axis("ep", chip * 2 + 1 - core)
    line = [lax.rem(chip + step, chips) * 2 + core for step in range(1, chips)]
    senders = [lax.rem(chip + chips - step, chips) * 2 + core for step in range(1, chips)]
    locals_ = []
    for part in range(parts):
        own = pltpu.make_async_copy(sources[part], targets[part].at[me], local_sem.at[part])
        own.start()
        locals_.append(own)
    enter([on_axis("ep", other) for other in line] + [partner])
    direct, copies = [], []
    for step, other in enumerate(line):
        for part in range(parts):
            direct.append(
                send(
                    sources[part],
                    targets[part].at[me],
                    send_sem.at[step, part],
                    recv_sem.at[step, part],
                    on_axis("ep", other),
                )
            )
    for part in range(parts):
        copies.append(
            send(
                sources[part],
                targets[part].at[me],
                send_sem.at[chips - 1, part],
                recv_sem.at[chips - 1, part],
                partner,
            )
        )
    for weight, result in zip(weights, results):
        result[...] = jnp.dot(
            tokens[...], weight[...], preferred_element_type=jnp.float32
        ).astype(result.dtype)
    for step, sender in enumerate(senders):
        for part in range(parts):
            direct[step * parts + part].wait_recv()
            copies.append(
                send(
                    targets[part].at[sender],
                    targets[part].at[sender],
                    send_sem.at[chips + step, part],
                    recv_sem.at[chips + step, part],
                    partner,
                )
            )
    for copy in locals_:
        copy.wait()
    for copy in direct:
        copy.wait_send()
    for copy in copies:
        copy.wait()


def first(arrays, tokens, weights, ident):
    count, parts = lax.axis_size("ep"), len(arrays)
    rows = tokens.shape[0]
    return pl.pallas_call(
        functools.partial(first_body, count),
        out_shape=[jax.ShapeDtypeStruct((count,) + a.shape, a.dtype) for a in arrays]
        + [jax.ShapeDtypeStruct((rows, w.shape[1]), jnp.bfloat16) for w in weights],
        in_specs=[VMEM] * (parts + 5),
        out_specs=[VMEM] * (parts + 4),
        scratch_shapes=[
            pltpu.SemaphoreType.DMA((count - 1, parts)),
            pltpu.SemaphoreType.DMA((count - 1, parts)),
            pltpu.SemaphoreType.DMA((parts,)),
        ],
        compiler_params=pltpu.CompilerParams(collective_id=ident, has_side_effects=True),
    )(*arrays, tokens, *weights)


def spread_body(count, tp_count, source, target, send_sem, recv_sem, local_sem):
    chips, width = count // 2, source.shape[1]
    me, own_tp = lax.axis_index("ep"), lax.axis_index("tp")
    chip, core = me // 2, lax.rem(me, 2)
    partner = (chip * 2 + 1 - core, own_tp)

    def place(row, col):
        return target.at[row, :, pl.ds(pl.multiple_of(col * width, width), width)]

    def chip_at(step):
        return lax.rem(chip + chips + step, chips) * 2 + core

    def tp_at(step):
        return lax.rem(own_tp + tp_count + step, tp_count)

    own = pltpu.make_async_copy(source, place(me, own_tp), local_sem)
    own.start()
    line = [(chip_at(step), own_tp) for step in range(1, chips)]
    plane = [(me, tp_at(step)) for step in range(1, tp_count)]
    enter(line + plane + [partner])

    def pair(line_step, plane_step, to_partner):
        return (
            send_sem.at[to_partner, line_step, plane_step],
            recv_sem.at[to_partner, line_step, plane_step],
        )

    direct, planar, copies = [], {}, []
    for step in range(1, chips):
        direct.append(send(source, place(me, own_tp), *pair(step, 0, 0), line[step - 1]))
    for step in range(1, tp_count):
        planar[(0, step)] = send(source, place(me, own_tp), *pair(0, step, 0), plane[step - 1])
    copies.append(send(source, place(me, own_tp), *pair(0, 0, 1), partner))
    for line_step in range(1, chips):
        direct[line_step - 1].wait_recv()
        block = place(chip_at(-line_step), own_tp)
        for step in range(1, tp_count):
            planar[(line_step, step)] = send(
                block, block, *pair(line_step, step, 0), plane[step - 1]
            )
        copies.append(send(block, block, *pair(line_step, 0, 1), partner))
    for line_step in range(chips):
        for step in range(1, tp_count):
            planar[(line_step, step)].wait_recv()
            block = place(chip_at(-line_step), tp_at(-step))
            copies.append(send(block, block, *pair(line_step, step, 1), partner))
    own.wait()
    for copy in direct:
        copy.wait_send()
    for copy in planar.values():
        copy.wait_send()
    for copy in copies:
        copy.wait()


def spread(block, ident):
    count, tp_count = lax.axis_size("ep"), lax.axis_size("tp")
    rows, width = block.shape
    return pl.pallas_call(
        functools.partial(spread_body, count, tp_count),
        out_shape=jax.ShapeDtypeStruct((count, rows, width * tp_count), block.dtype),
        in_specs=[VMEM],
        out_specs=VMEM,
        scratch_shapes=[
            pltpu.SemaphoreType.DMA((2, count // 2, tp_count)),
            pltpu.SemaphoreType.DMA((2, count // 2, tp_count)),
            pltpu.SemaphoreType.DMA,
        ],
        compiler_params=pltpu.CompilerParams(collective_id=ident, has_side_effects=True),
    )(block)


def side_by_side(gathered):
    return jnp.concatenate([gathered[i] for i in range(gathered.shape[0])], -1)


def row_moments(values, ident):
    sums = jnp.stack([jnp.sum(values, -1), jnp.sum(values * values, -1)])
    (every,) = gather([sums], "tp", ident)
    totals = jnp.sum(every, 0)
    return totals[0][:, None], totals[1][:, None]


def on_device(
    tokens,
    retention_state,
    lengths,
    query_weight,
    key_weight,
    value_weight,
    gate_weight,
    out_weight,
    first_gain,
    routing,
    route_weight,
    expert_gate,
    expert_up,
    expert_down,
    shared_gate,
    shared_up,
    shared_down,
    side_gate,
    side_up,
    side_down,
    side_switch,
    second_gain,
):
    seq_rows = tokens.shape[0]
    model_width = tokens.shape[1]
    head_count = retention_state.shape[1]
    col_count = out_weight.shape[1]
    ep_count = lax.axis_size("ep")
    tp_rank = lax.axis_index("tp")
    ep_rank = lax.axis_index("ep")
    col_start = tp_rank * col_count
    side_width = side_gate.shape[1]
    side_part = jnp.concatenate([side_gate, side_up], 1)
    side_both, every_route, every_weight, *projections = first(
        [side_part, routing.T, route_weight.T],
        tokens,
        [query_weight, key_weight, value_weight, gate_weight],
        0,
    )
    side_both = side_both.reshape(model_width, 2 * side_width)
    mixed_heads, new_state = retain(
        retention_state, lengths, projections, tp_rank * head_count
    )
    (every_mixed,) = gather([mixed_heads], "tp", 1)
    mixing = jnp.dot(
        side_by_side(every_mixed),
        out_weight,
        preferred_element_type=jnp.float32,
    )
    own_cols = lax.dynamic_slice_in_dim(tokens, col_start, col_count, 1).astype(jnp.float32)
    pre_first = RESIDUAL_SCALE * own_cols + mixing
    first_sum, first_square = row_moments(pre_first, 2)
    row_mean = first_sum / model_width
    square = first_square / model_width
    own_gain = lax.dynamic_slice_in_dim(first_gain, col_start, col_count, 0)
    normed_cols = (
        (pre_first - row_mean) * lax.rsqrt(square - row_mean * row_mean + NORM_EPS) * own_gain
    ).astype(jnp.bfloat16)
    every_rows = spread(normed_cols, 3)
    normed_full = lax.dynamic_index_in_dim(every_rows, ep_rank, 0, keepdims=False)
    every_rows = every_rows.reshape(ep_count * seq_rows, model_width)

    local_experts = expert_gate.shape[0]
    top_count = routing.shape[1]
    expert_count = local_experts * ep_count
    capacity = (3 * seq_rows * top_count + expert_count - 1) // expert_count
    total_rows = ep_count * seq_rows
    route_all = jnp.transpose(every_route, (1, 0, 2)).reshape(top_count, total_rows)
    weight_all = jnp.transpose(every_weight, (1, 0, 2)).reshape(top_count, total_rows)
    local_ids = ep_rank * local_experts + jnp.arange(local_experts, dtype=jnp.int32)
    named = route_all[None, :, :] == local_ids[:, None, None]
    member = jnp.any(named, 1)
    pair_weight = jnp.sum(jnp.where(named, weight_all[None, :, :], 0.0), 1)
    index = jnp.arange(total_rows, dtype=jnp.int32)
    group = index // seq_rows
    earlier = ((index[:, None] < index[None, :]) & (group[:, None] == group[None, :])).astype(
        jnp.bfloat16
    )
    before = jnp.dot(
        member.astype(jnp.bfloat16), earlier, preferred_element_type=jnp.float32
    ).astype(jnp.int32)
    slot = jnp.where(member, group[None, :] * capacity + before, -1)
    slot_total = ep_count * capacity
    hit = slot[:, None, :] == jnp.arange(slot_total, dtype=jnp.int32)[None, :, None]
    table = hit.astype(jnp.bfloat16).reshape(local_experts * slot_total, total_rows)
    slot_weight = jnp.sum(jnp.where(hit, pair_weight[:, None, :], 0.0), -1, keepdims=True)
    chosen = (
        jnp.dot(table, every_rows, preferred_element_type=jnp.float32)
        .astype(jnp.bfloat16)
        .reshape(local_experts, slot_total, model_width)
    )
    gate_part = jnp.einsum("jcd,jdf->jcf", chosen, expert_gate, preferred_element_type=jnp.float32)
    up_part = jnp.einsum("jcd,jdf->jcf", chosen, expert_up, preferred_element_type=jnp.float32)
    hidden = (jax.nn.silu(gate_part) * up_part * slot_weight).astype(jnp.bfloat16)

    side_pre = jnp.dot(normed_full, side_both, preferred_element_type=jnp.float32)
    side_hidden = (jax.nn.silu(side_pre[:, :side_width]) * side_pre[:, side_width:]).astype(
        jnp.bfloat16
    )
    shared_hidden = (
        jax.nn.silu(jnp.dot(normed_full, shared_gate, preferred_element_type=jnp.float32))
        * jnp.dot(normed_full, shared_up, preferred_element_type=jnp.float32)
    ).astype(jnp.bfloat16)
    hidden_blocks, shared_blocks, side_blocks = gather(
        [hidden.reshape(local_experts * slot_total, -1), shared_hidden, side_hidden], "tp", 4
    )
    hidden_all = side_by_side(hidden_blocks).reshape(local_experts, slot_total, -1)
    result = (
        jnp.einsum("jcf,jfd->jcd", hidden_all, expert_down, preferred_element_type=jnp.float32)
        .astype(jnp.bfloat16)
        .reshape(local_experts * slot_total, col_count)
    )
    summed = (
        lax.dot_general(
            table, result, (((0,), (0,)), ((), ())), preferred_element_type=jnp.float32
        )
        .astype(jnp.bfloat16)
        .reshape(ep_count, seq_rows, col_count)
    )
    returned = scatter(summed, 5)
    routed = jnp.sum(returned.astype(jnp.float32), 0)
    shared_out = jnp.dot(
        side_by_side(shared_blocks), shared_down, preferred_element_type=jnp.float32
    )
    side_out = jnp.dot(side_by_side(side_blocks), side_down, preferred_element_type=jnp.float32)
    switch = jax.nn.sigmoid(
        jnp.sum(normed_full.astype(jnp.float32) * side_switch.astype(jnp.float32)[None, :], -1)
    )
    pre_second = (
        RESIDUAL_SCALE * normed_cols.astype(jnp.float32)
        + routed
        + shared_out
        + switch[:, None] * side_out
    )
    second_sum, second_square = row_moments(pre_second, 6)
    mean_second = second_sum / model_width
    square_second = second_square / model_width
    output = (
        (pre_second - mean_second)
        * lax.rsqrt(square_second - mean_second * mean_second + NORM_EPS)
        * second_gain
    ).astype(jnp.bfloat16)
    return (output, new_state)


def solution(mesh):
    return jax.shard_map(
        on_device,
        mesh=mesh,
        in_specs=(
            P("ep", None),
            P("ep", "tp", None, None),
            P("ep"),
            P(None, "tp"),
            P(None, "tp"),
            P(None, "tp"),
            P(None, "tp"),
            P(None, "tp"),
            P(),
            P("ep", None),
            P("ep", None),
            P("ep", None, "tp"),
            P("ep", None, "tp"),
            P("ep", None, "tp"),
            P(None, "tp"),
            P(None, "tp"),
            P(None, "tp"),
            P("ep", "tp"),
            P("ep", "tp"),
            P(None, "tp"),
            P(),
            P("tp"),
        ),
        out_specs=(P("ep", "tp"), P("ep", "tp", None, None)),
        check_vma=False,
    )
```

profile of v0, /device:TPU:0, one launch (start us, length us, event | category | flops | bytes accessed | tf_op | source)
XLA Modules:
  0.0 123.5 jit_solution(15533541414120755268)
XLA Ops:
  1.5 1.3 %dynamic_slice.11 = f32[512]{0:T(512)} dynamic-slice(f32[2048]{0:T(1024)} %param.30, s32[]{:T(128)S(6)} %select_n.38), dynamic_slice_sizes={512} | dynamic-slice | bytes 4100 | tf_op jit(solution)/shard_map/dynamic_slice | solution.py:401
  4.4 0.9 copy.39
  5.3 0.9 copy.40
  6.9 15.6 %shard_map.221 = (bf16[8,256,128]{2,1,0:T(8,128)(2,1)}, s32[8,4,48]{2,1,0:T(4,128)}, f32[8,4,48]{2,1,0:T(4,128)}, bf16[48,256]{1,0:T(8,128)(2,1)}, bf16[48,256]{...) custom-call(bf16[256,128]{1,0:T(8,128)(2,1)} %pad_maximum_fusion.1.refs_0_, s32[4,48]{1,0:T(4,128)} %bitcast.101, ...), custom_call_target="tpu_custom_call" | custom-call | tf_op jit(solution)/shard_map/pallas_call | solution.py:248
  26.3 0.8 reshape.296
  27.1 0.8 reshape.305
  30.2 9.2 %multiply_add_fusion = (f32[48,4,64,64]{3,2,1,0:T(8,128)}, f32[48,4,64]{2,1,0:T(4,128)S(1)}) fusion(f32[48,4,64,64]{3,2,1,0:T(8,128)} %param.23, f32[48,4,64]{2,1,0:T(4,128)S(1)} %reshape.296, f32[48,4,64]{2,1,0:T(4,128)S(1)} %get-tuple-element.27, f32[4]{0:T(128)} %copy-done.14, f32[48,4,64]{2,1,0:T(4,128)S(1)} %get-tuple-element.28), kind=kLoop, calls=%fused_computation | loop fusion | flops 3919872 | bytes 6488080 | tf_op jit(solution)/shard_map/add | solution.py:59
  40.0 1.4 %fusion.53.refs_0_ = bf16[48,256]{1,0:T(8,128)(2,1)} fusion(bf16[48,256]{1,0:T(8,128)(2,1)} %get-tuple-element.15, f32[48,256]{1,0:T(8,128)S(1)} %mul.334, f32[48,256]{1,0:T(8,128)S(1)} %reduce_sum.121, f32[48,256]{1,0:T(8,128)} %mul.320, f32[256]{0:T(256)} %mul.324, bf16[48,256]{1,0:T(8,128)(2,1)} %get-tuple-element.14), kind=kLoop, calls=%fused_computation.76 | loop fusion | flops 147456 | bytes 222208 | tf_op jit(solution)/shard_map/convert_element_type | solution.py:65
  41.4 6.5 %shard_map.222 = bf16[4,48,256]{2,1,0:T(8,128)(2,1)} custom-call(bf16[48,256]{1,0:T(8,128)(2,1)} %fusion.53.refs_0_), custom_call_target="tpu_custom_call" | custom-call | tf_op jit(solution)/shard_map/pallas_call | solution.py:130
  48.7 1.2 fusion.79
  50.5 5.8 %shard_map.223 = f32[4,2,48]{2,1,0:T(2,128)} custom-call(f32[2,48]{1,0:T(2,128)} %pad_maximum_fusion.2.refs_0_), custom_call_target="tpu_custom_call" | custom-call | tf_op jit(solution)/shard_map/pallas_call | solution.py:130
  57.8 17.7 %shard_map.224 = bf16[8,48,2048]{2,1,0:T(8,128)(2,1)} custom-call(bf16[48,512]{1,0:T(8,128)(2,1)} %multiply_convert_fusion.1.source), custom_call_target="tpu_custom_call" | custom-call | tf_op jit(solution)/shard_map/pallas_call | solution.py:321
  75.5 1.5 %fusion.27 = f32[48,128]{1,0:T(8,128)S(1)} fusion(bf16[2048,128]{1,0:T(8,128)(2,1)} %bitcast.91, bf16[8,48,2048]{2,1,0:T(8,128)(2,1)} %shard_map.224, s32[]{:T(128)S(6)} %select_n.43), kind=kOutput, calls=%fused_computation.35 | convolution fusion | flops 25165824 | bytes 745476 | tf_op jit(solution)/shard_map/dot_general | solution.py:442
  77.7 1.1 multiply_reduce_fusion.1
  78.8 1.4 %fusion.30 = f32[48,128]{1,0:T(8,128)S(1)} fusion(bf16[2048,128]{1,0:T(8,128)(2,1)} %param.36, bf16[8,48,2048]{2,1,0:T(8,128)(2,1)} %shard_map.224, s32[]{:T(128)S(6)} %select_n.43), kind=kOutput, calls=%fused_computation.38 | convolution fusion | flops 25165824 | bytes 745476 | tf_op jit(solution)/shard_map/dot_general | solution.py:447
  80.1 1.7 %fusion.4.refs_1_ = bf16[48,128]{1,0:T(8,128)(2,1)} fusion(bf16[2048,128]{1,0:T(8,128)(2,1)S(1)} %copy-done.4, bf16[8,48,2048]{2,1,0:T(8,128)(2,1)} %shard_map.224, s32[]{:T(128)S(6)} %select_n.43, f32[48,128]{1,0:T(8,128)S(1)} %fusion.30), kind=kOutput, calls=%fused_computation.14 | convolution fusion | flops 25202688 | bytes 757764 | tf_op jit(solution)/shard_map/dot_general | solution.py:448
  81.9 1.4 %convolution_convert_fusion = bf16[576,2048]{1,0:T(8,128)(2,1)S(1)} fusion(pred[576,384]{1,0:T(8,128)(4,1)S(1)} %bitcast.93, bf16[384,2048]{1,0:T(8,128)(2,1)S(1)} %bitcast.88), kind=kOutput, calls=%fused_computation.2 | convolution fusion | flops 907149312 | bytes 4153344 | tf_op jit(solution)/shard_map/dot_general | solution.py:434
  85.1 1.5 %fusion.2 = bf16[4,144,128]{2,1,0:T(8,128)(2,1)} fusion(bf16[4,144,2048]{2,1,0:T(8,128)(2,1)S(1)} %bitcast.90, bf16[4,2048,128]{2,1,0:T(8,128)(2,1)S(1)} %copy-done.18, f32[4,144,128]{2,1,0:T(8,128)S(1)} %fusion.81, f32[4,144]{1,0:T(4,128)S(1)} %copy-done.16), kind=kOutput, calls=%fused_computation.8 | convolution fusion | flops 302505984 | bytes 4901120 | tf_op jit(solution)/shard_map/jcd,jdf->jcf/dot_general | solution.py:439
  86.6 12.9 %shard_map.225 = (bf16[4,576,128]{2,1,0:T(8,128)(2,1)}, bf16[4,48,128]{2,1,0:T(8,128)(2,1)}, bf16[4,48,64]{2,1,0:T(8,128)(2,1)}) custom-call(bf16[576,128]{1,0:T(8,128)(2,1)} %bitcast.98, bf16[48,128]{1,0:T(8,128)(2,1)} %fusion.4.refs_1_, bf16[48,64]{1,0:T(8,128)(2,1)} %fusion.55.refs_2_), custom_call_target="tpu_custom_call" | custom-call | tf_op jit(solution)/shard_map/pallas_call | solution.py:130
  99.5 1.2 fusion.80
  100.7 1.6 %fusion = bf16[384,512]{1,0:T(8,128)(2,1)} fusion(bf16[4,512,512]{2,1,0:T(8,128)(2,1)S(1)} %copy-done, bf16[4,144,128]{2,1,0:T(8,128)(2,1)S(1)} %bitcast.95, bf16[4,144,128]{2,1,0:T(8,128)(2,1)S(1)} %bitcast.96, bf16[4,144,128]{2,1,0:T(8,128)(2,1)S(1)} %bitcast.97, bf16[4,144,128]{2,1,0:T(8,128)(2,1)S(1)} %bitcast.94, s32[4,384]{1,0:T(4,128)S(1)} %fusion.6), kind=kOutput, calls=%fused_computation.5 | convolution fusion | flops 531554304 | bytes 3086336 | tf_op jit(solution)/shard_map/dot_general | solution.py:460
  102.3 11.8 %shard_map.226 = bf16[8,48,512]{2,1,0:T(8,128)(2,1)} custom-call(bf16[8,48,512]{2,1,0:T(8,128)(2,1)} %bitcast.92), custom_call_target="tpu_custom_call" | custom-call | tf_op jit(solution)/shard_map/pallas_call | solution.py:167
  114.1 1.1 convert_reduce_fusion
  116.3 5.8 %shard_map.227 = f32[4,2,48]{2,1,0:T(2,128)} custom-call(f32[2,48]{1,0:T(2,128)} %pad_maximum_fusion.3.refs_0_), custom_call_target="tpu_custom_call" | custom-call | tf_op jit(solution)/shard_map/pallas_call | solution.py:130
  (85 shorter events, 17.4 us)
Async XLA Ops:
  0.6 100.0 %copy-start = (bf16[4,512,512]{2,1,0:T(8,128)(2,1)S(1)}, bf16[4,512,512]{2,1,0:T(8,128)(2,1)}, u32[]{:S(2)}) copy-start(bf16[4,512,512]{2,1,0:T(8,128)(2,1)} %param.35) | copy-start | bytes 6291460
  0.7 2.2 %copy-start.14 = (f32[4]{0:T(128)}, f32[4]{0:T(128)S(1)}, u32[]{:S(2)}) copy-start(f32[4]{0:T(128)S(1)} %power_subtract_fusion) | copy-start | bytes 52
  28.5 1.7 %copy-start.9 = (f32[48,4]{1,0:T(8,128)}, f32[48,4]{1,0:T(8,128)S(1)}, u32[]{:S(2)}) copy-start(f32[48,4]{1,0:T(8,128)S(1)} %get-tuple-element.26) | copy-start | bytes 2308
  30.2 9.2 %copy-start.10 = (f32[48,4]{1,0:T(8,128)S(1)}, f32[48,4]{1,0:T(8,128)}, u32[]{:S(2)}) copy-start(f32[48,4]{1,0:T(8,128)} %copy-done.9) | copy-start | bytes 2308
  30.2 9.2 %copy-start.15 = (f32[4]{0:T(128)S(1)}, f32[4]{0:T(128)}, u32[]{:S(2)}) copy-start(f32[4]{0:T(128)} %copy-done.14) | copy-start | bytes 52
  30.2 18.5 %copy-start.3 = (bf16[1024,512]{1,0:T(8,128)(2,1)S(1)}, bf16[1024,512]{1,0:T(8,128)(2,1)}, u32[]{:S(2)}) copy-start(bf16[1024,512]{1,0:T(8,128)(2,1)} %param.29) | copy-start | bytes 3145732
  39.4 17.7 %copy-start.13 = (f32[512]{0:T(512)S(1)}, f32[512]{0:T(512)}, u32[]{:S(2)}) copy-start(f32[512]{0:T(512)} %dynamic_slice.11) | copy-start | bytes 6148
  49.9 30.2 %copy-start.4 = (bf16[2048,128]{1,0:T(8,128)(2,1)S(1)}, bf16[2048,128]{1,0:T(8,128)(2,1)}, u32[]{:S(2)}) copy-start(bf16[2048,128]{1,0:T(8,128)(2,1)} %param.37) | copy-start | bytes 1572868
  57.8 24.1 %copy-start.8 = (pred[4,144,384]{2,1,0:T(8,128)(4,1)S(1)}, pred[4,144,384]{2,1,0:T(8,128)(4,1)}, u32[]{:S(2)}) copy-start(pred[4,144,384]{2,1,0:T(8,128)(4,1)} %iota_compare_fusion) | copy-start | bytes 663556
  75.5 6.4 %copy-start.1 = (bf16[8,48,2048]{2,1,0:T(8,128)(2,1)S(1)}, bf16[8,48,2048]{2,1,0:T(8,128)(2,1)}, u32[]{:S(2)}) copy-start(bf16[8,48,2048]{2,1,0:T(8,128)(2,1)} %shard_map.224) | copy-start | bytes 4718596
  81.9 1.6 %copy-start.2 = (bf16[4,2048,128]{2,1,0:T(8,128)(2,1)S(1)}, bf16[4,2048,128]{2,1,0:T(8,128)(2,1)}, u32[]{:S(2)}) copy-start(bf16[4,2048,128]{2,1,0:T(8,128)(2,1)} %param.33) | copy-start | bytes 6291460
  83.5 0.8 copy-start.16
  83.5 1.6 %copy-start.18 = (bf16[4,2048,128]{2,1,0:T(8,128)(2,1)S(1)}, bf16[4,2048,128]{2,1,0:T(8,128)(2,1)}, u32[]{:S(2)}) copy-start(bf16[4,2048,128]{2,1,0:T(8,128)(2,1)} %param.34) | copy-start | bytes 6291460
  100.7 14.4 %copy-start.12 = (bf16[4,48,128]{2,1,0:T(8,128)(2,1)S(1)}, bf16[4,48,128]{2,1,0:T(8,128)(2,1)}, u32[]{:S(2)}) copy-start(bf16[4,48,128]{2,1,0:T(8,128)(2,1)} %get-tuple-element.20) | copy-start | bytes 147460
  100.7 14.4 %copy-start.5 = (bf16[512,512]{1,0:T(8,128)(2,1)S(1)}, bf16[512,512]{1,0:T(8,128)(2,1)}, u32[]{:S(2)}) copy-start(bf16[512,512]{1,0:T(8,128)(2,1)} %param.38) | copy-start | bytes 1572868
  100.7 14.4 %copy-start.6 = (bf16[48,512]{1,0:T(8,128)(2,1)S(1)}, bf16[48,512]{1,0:T(8,128)(2,1)}, u32[]{:S(2)}) copy-start(bf16[48,512]{1,0:T(8,128)(2,1)} %multiply_convert_fusion.1.source) | copy-start | bytes 147460
  102.3 13.1 %copy-start.11 = (bf16[4,48,64]{2,1,0:T(8,128)(2,1)S(1)}, bf16[4,48,64]{2,1,0:T(8,128)(2,1)}, u32[]{:S(2)}) copy-start(bf16[4,48,64]{2,1,0:T(8,128)(2,1)} %get-tuple-element.21) | copy-start | bytes 73732
  102.3 13.1 %copy-start.7 = (bf16[256,512]{1,0:T(8,128)(2,1)S(1)}, bf16[256,512]{1,0:T(8,128)(2,1)}, u32[]{:S(2)}) copy-start(bf16[256,512]{1,0:T(8,128)(2,1)} %param.41) | copy-start | bytes 786436
  102.3 20.5 %copy-start.17 = (f32[512]{0:T(512)S(1)}, f32[512]{0:T(512)}, u32[]{:S(2)}) copy-start(f32[512]{0:T(512)} %param.43) | copy-start | bytes 6148
where the time goes:
time: 125 us; the launch traced here: 124 us
  Pallas kernels  76.2 us (61%)
  other arithmetic  22.4 us (18%)
  local copies, waits for them, and re-layouts  12.2 us (10%)
  matrix products  11.8 us (9%)
    pallas_call x4, Pallas kernels, gather(): pl.pallas_call(functools.partial(gather_body, axis, count, parts), out_sh...  31.1 us
    pallas_call x1, Pallas kernels, spread(): pl.pallas_call(functools.partial(spread_body, count, tp_count), out_shape...  17.7 us
    pallas_call x1, Pallas kernels, first(): pl.pallas_call(functools.partial(first_body, count), out_shape=[jax.Shape...  15.6 us
    pallas_call x1, Pallas kernels, scatter(): pl.pallas_call(functools.partial(scatter_body, count), out_shape=jax.Shap...  11.8 us
    add x1, other arithmetic, retain(): decays[None, :, None, None] * retention_state  9.16 us
    unnamed x40, local copies, waits for them, and re-layouts  2.83 us

commit v1 on v0

--- a/solution.py
+++ b/solution.py
@@ -2,6 +2,7 @@
 
 import jax
 import jax.numpy as jnp
+import numpy as np
 from jax import lax
 from jax.experimental import pallas as pl
 from jax.experimental.pallas import tpu as pltpu
@@ -343,7 +344,708 @@
     return totals[0][:, None], totals[1][:, None]
 
 
-def on_device(
+ANY = pl.BlockSpec(memory_space=pl.ANY)
+
+
+def dot(a, b):
+    return jnp.dot(a, b, preferred_element_type=jnp.float32)
+
+
+def silu(x):
+    return x / (1.0 + jnp.exp(-x))
+
+
+def fetch(source, target, sem):
+    copy = pltpu.make_async_copy(source, target, sem)
+    copy.start()
+    return copy
+
+
+def rotated(x, cosine, sine, half):
+    width = x.shape[1]
+    lane = lax.broadcasted_iota(jnp.int32, x.shape, 1)
+    first = (lane & (2 * half - 1)) < half
+    later = pltpu.roll(x, width - half, 1)
+    sooner = pltpu.roll(x, half, 1)
+    return x * cosine + jnp.where(first, -later, sooner) * sine
+
+
+def retain_body(
+    chunk,
+    tokens_in,
+    lengths,
+    frequency,
+    query_in,
+    key_in,
+    value_in,
+    gate_in,
+    state_in,
+    mixed,
+    state_out,
+    tokens,
+    weights,
+    state,
+    queries,
+    keys,
+    values,
+    carried,
+    weight_sem,
+    state_sem,
+    out_sem,
+):
+    rows, heads, width = state.shape[0], state.shape[1], state.shape[2]
+    chunks = rows // chunk
+    tokens_copy = fetch(tokens_in, tokens, weight_sem.at[4])
+    copies = [
+        fetch(source, weights.at[i], weight_sem.at[i])
+        for i, source in enumerate([query_in, key_in, value_in, gate_in])
+    ]
+    for i in range(chunks):
+        piece = pl.ds(i * chunk, chunk)
+        fetch(state_in.at[piece], state.at[piece], state_sem.at[i])
+
+    row = lax.broadcasted_iota(jnp.int32, (rows, rows), 0)
+    col = lax.broadcasted_iota(jnp.int32, (rows, rows), 1)
+    position = jnp.sum(
+        jnp.where(row == col, lengths[...].astype(jnp.float32), 0.0), 1, keepdims=True
+    )
+    angles = position * frequency[...]
+    cosine, sine = jnp.cos(angles), jnp.sin(angles)
+    first_head = lax.axis_index("tp") * heads
+
+    tokens_copy.wait()
+
+    def project(i):
+        copies[i].wait()
+        return dot(tokens[...], weights[i]).astype(jnp.bfloat16).astype(jnp.float32)
+
+    def head_of(x, head):
+        return x[:, head * width : (head + 1) * width]
+
+    query = rotated(project(0), cosine, sine, width // 2)
+    queries[...] = query
+    key = rotated(project(1), cosine, sine, width // 2) * width ** (-0.5)
+    keys[...] = key
+    value = project(2)
+    for head in range(heads):
+        values[head] = head_of(value, head)
+    gate = project(3)
+    decays = []
+    for head in range(heads):
+        index = jnp.full((1, width), first_head + head, jnp.int32).astype(jnp.float32)
+        decays.append(1.0 - jnp.exp2(-5.0 - 7.0 * index / (HEADS - 1)))
+
+    def step(i, carry):
+        base = pl.multiple_of(i * chunk, chunk)
+        piece = pl.ds(base, chunk)
+        pltpu.make_async_copy(state_in.at[piece], state.at[piece], state_sem.at[i]).wait()
+        query_cols = jnp.transpose(queries[piece, :])
+        key_cols = jnp.transpose(keys[piece, :])
+        for at in range(chunk):
+            for head in range(heads):
+                span = slice(head * width, (head + 1) * width)
+                old = state[base + at, head]
+                q_col = query_cols[span, at : at + 1]
+                k_col = key_cols[span, at : at + 1]
+                v_row = values[head, pl.ds(base + at, 1), :]
+                carried[head, pl.ds(base + at, 1), :] = jnp.sum(q_col * old, 0, keepdims=True)
+                state[base + at, head] = decays[head] * old + k_col * v_row
+        pltpu.make_async_copy(state.at[piece], state_out.at[piece], out_sem.at[i]).start()
+        return carry
+
+    lax.fori_loop(0, chunks, step, 0)
+    both = query * key
+    parts = []
+    for head in range(heads):
+        own = jnp.sum(head_of(both, head), -1, keepdims=True) * values[head]
+        result = own + decays[head] * carried[head]
+        scale = lax.rsqrt(jnp.mean(result * result, -1, keepdims=True) + GROUP_EPS)
+        parts.append(result * scale)
+    mixed[...] = (jnp.concatenate(parts, 1) * silu(gate)).astype(mixed.dtype)
+    for i in range(chunks):
+        piece = pl.ds(i * chunk, chunk)
+        pltpu.make_async_copy(state.at[piece], state_out.at[piece], out_sem.at[i]).wait()
+
+
+def retain_kernel(tokens, lengths, frequency, weights, state):
+    rows, heads, width = state.shape[0], state.shape[1], state.shape[2]
+    chunk = 8
+    cols = heads * width
+    return pl.pallas_call(
+        functools.partial(retain_body, chunk),
+        out_shape=[
+            jax.ShapeDtypeStruct((rows, cols), jnp.bfloat16),
+            jax.ShapeDtypeStruct(state.shape, state.dtype),
+        ],
+        in_specs=[ANY, VMEM, VMEM] + [ANY] * 5,
+        out_specs=[VMEM, ANY],
+        scratch_shapes=[
+            pltpu.VMEM(tokens.shape, tokens.dtype),
+            pltpu.VMEM((4,) + weights[0].shape, weights[0].dtype),
+            pltpu.VMEM(state.shape, state.dtype),
+            pltpu.VMEM((rows, cols), jnp.float32),
+            pltpu.VMEM((rows, cols), jnp.float32),
+            pltpu.VMEM((heads, rows, width), jnp.float32),
+            pltpu.VMEM((heads, rows, width), jnp.float32),
+            pltpu.SemaphoreType.DMA((5,)),
+            pltpu.SemaphoreType.DMA((rows // chunk,)),
+            pltpu.SemaphoreType.DMA((rows // chunk,)),
+        ],
+    )(tokens, lengths, frequency, *weights, state)
+
+
+def mixer_body(
+    dims,
+    mixed,
+    tokens,
+    routes,
+    route_weights,
+    first_gain,
+    second_gain,
+    side_switch,
+    out_in,
+    gate_in,
+    up_in,
+    down_in,
+    shared_gate_in,
+    shared_up_in,
+    shared_down_in,
+    side_gate_in,
+    side_up_in,
+    side_down_in,
+    output,
+    mixed_all,
+    route_all,
+    weight_all,
+    rows_all,
+    normed,
+    own_normed,
+    info,
+    info_cols,
+    hidden_all,
+    pair_out,
+    pair_in,
+    line_out,
+    line_in,
+    total,
+    side_out,
+    side_in,
+    late_all,
+    stats,
+    out_w,
+    gate_up_w,
+    down_w,
+    shared_w,
+    shared_down_w,
+    side_w,
+    side_down_w,
+    weight_sem,
+    head_sems,
+    route_sems,
+    row_sems,
+    hidden_sems,
+    back_sems,
+    side_sems,
+    late_sems,
+    stat_sems,
+):
+    chips, tps, capacity = dims
+    steps = chips
+    rows, model = tokens.shape
+    cols = model // tps
+    half = cols // 2
+    experts, hidden_width = gate_in.shape[0], gate_in.shape[2]
+    slots = hidden_all.shape[3]
+    side_width = side_gate_in.shape[0]
+    side_rows = side_gate_in.shape[1]
+    tp = lax.axis_index("tp")
+    ep = lax.axis_index("ep")
+    chip, core = ep // 2, lax.rem(ep, 2)
+    partner = (chip * 2 + 1 - core, tp)
+    low, high = lax.rem(tp, 2), tp // 2
+    tp_x = high * 2 + 1 - low
+    tp_y = (1 - high) * 2 + low
+    tp_d = (1 - high) * 2 + 1 - low
+    plane = [(ep, tp_x), (ep, tp_y), (ep, tp_d)]
+
+    def chip_at(step):
+        if step == 0:
+            return chip
+        if step == 1:
+            return chip + 1 - 2 * lax.rem(chip, 2)
+        if step == 2:
+            return lax.rem(chip + 2, 4)
+        return 3 - chip
+
+    others = []
+    for step in range(1, steps):
+        others += [(chip_at(step) * 2 + core, tp), (chip_at(step) * 2 + 1 - core, tp)]
+    others.append(partner)
+
+    loads = {}
+
+    def load(name, source, target, index):
+        loads.setdefault(name, []).append(fetch(source, target, weight_sem.at[index]))
+
+    def ready(name):
+        for copy in loads.pop(name):
+            copy.wait()
+
+    load("out", out_in, out_w, 0)
+    for e in range(experts):
+        load("gate_up", gate_in.at[e], gate_up_w.at[e, :, pl.ds(0, hidden_width)], 1 + 2 * e)
+        load(
+            "gate_up",
+            up_in.at[e],
+            gate_up_w.at[e, :, pl.ds(hidden_width, hidden_width)],
+            2 + 2 * e,
+        )
+    base = 1 + 2 * experts
+    shared_width = shared_gate_in.shape[1]
+    load("side", side_gate_in, side_w.at[pl.ds(0, side_width)], base)
+    load("side", side_up_in, side_w.at[pl.ds(side_width, side_width)], base + 1)
+    load("shared", shared_gate_in, shared_w.at[:, pl.ds(0, shared_width)], base + 2)
+    load("shared", shared_up_in, shared_w.at[:, pl.ds(shared_width, shared_width)], base + 3)
+    load("down", down_in, down_w, base + 4)
+    load("late", shared_down_in, shared_down_w, base + 5)
+    load("late", side_down_in, side_down_w, base + 6)
+
+    pending = []
+
+    def push(source, target, sems, index, peer):
+        copy = send(source, target, sems.at[(0,) + index], sems.at[(1,) + index], peer)
+        pending.append(copy)
+        return copy
+
+    enter(plane + others)
+
+    mixed_copies = [push(mixed, mixed_all.at[tp], head_sems, (i,), p) for i, p in enumerate(plane)]
+    route_copies = []
+    for i, other in enumerate(others):
+        route_copies.append(push(routes, route_all.at[ep], route_sems, (i, 0), other))
+        route_copies.append(push(route_weights, weight_all.at[ep], route_sems, (i, 1), other))
+    route_all[ep] = routes[...]
+    weight_all[ep] = route_weights[...]
+
+    def head_rows(index):
+        width = mixed.shape[1]
+        return out_w[pl.ds(pl.multiple_of(index * width, width), width), :]
+
+    ready("out")
+    own_cols = tokens[:, pl.ds(pl.multiple_of(tp * cols, cols), cols)].astype(jnp.float32)
+    pre_first = RESIDUAL_SCALE * own_cols + dot(mixed[...], head_rows(tp))
+    for copy, index in zip(mixed_copies, [tp_x, tp_y, tp_d]):
+        copy.wait_recv()
+        pre_first = pre_first + dot(mixed_all[index], head_rows(index))
+    for part in range(2):
+        rows_all[ep, 2 * tp + part] = pre_first[:, part * half : (part + 1) * half].astype(
+            jnp.bfloat16
+        )
+
+    def block(step, index):
+        return rows_all.at[chip_at(step) * 2 + core, pl.ds(2 * index, 2)]
+
+    def piece(step, index, part):
+        return rows_all.at[chip_at(step) * 2 + core, 2 * index + part]
+
+    line = {}
+    flat = {}
+    across = {}
+    shared_rows = {}
+
+    def push_rows(ref, step, kind, peer):
+        return push(ref, ref, row_sems, (step, kind), peer)
+
+    def spread(step):
+        if step > 0:
+            line[step].wait_recv()
+        ref = block(step, tp)
+        flat[step] = (push_rows(ref, step, 1, plane[0]), push_rows(ref, step, 2, plane[1]))
+        shared_rows[step] = [push_rows(ref, step, 3, partner)]
+
+    def relay(step):
+        by_x, by_y = flat[step]
+        by_x.wait_recv()
+        first_half = push_rows(piece(step, tp_x, 0), step, 4, plane[1])
+        shared_rows[step].append(push_rows(block(step, tp_x), step, 5, partner))
+        by_y.wait_recv()
+        second_half = push_rows(piece(step, tp_y, 1), step, 6, plane[0])
+        shared_rows[step].append(push_rows(block(step, tp_y), step, 7, partner))
+        across[step] = (first_half, second_half)
+
+    def corner(step):
+        for part in range(2):
+            across[step][part].wait_recv()
+            shared_rows[step].append(push_rows(piece(step, tp_d, part), step, 8 + part, partner))
+
+    def arrive(step):
+        for copy in shared_rows[step]:
+            copy.wait_recv()
+
+    for step in range(1, steps):
+        line[step] = push(
+            block(0, tp), block(0, tp), row_sems, (step, 0), (chip_at(step) * 2 + core, tp)
+        )
+    spread(0)
+
+    for copy in route_copies:
+        copy.wait_recv()
+    wide = experts * rows
+
+    def expert_of(index):
+        return sum(jnp.where(index >= e * rows, 1, 0) for e in range(1, experts))
+
+    group_lane = expert_of(lax.broadcasted_iota(jnp.int32, (1, wide), 1))
+    expert_lane = ep * experts + group_lane
+    info[...] = jnp.zeros_like(info)
+    eps = route_all.shape[0]
+    for g in range(eps):
+        ids = jnp.concatenate([route_all[g]] * experts, 1)
+        hits = ids == expert_lane
+        scales = jnp.concatenate([weight_all[g]] * experts, 1)
+        info[g : g + 1, 0:wide] = jnp.sum(jnp.where(hits, 1.0, 0.0), 0, keepdims=True)
+        info[eps + g : eps + g + 1, 0:wide] = jnp.sum(
+            jnp.where(hits, scales, 0.0), 0, keepdims=True
+        )
+    member = info[0:eps, 0:wide]
+    sooner = lax.broadcasted_iota(jnp.int32, (wide, wide), 0)
+    later = lax.broadcasted_iota(jnp.int32, (wide, wide), 1)
+    earlier = jnp.where(
+        (sooner < later) & (expert_of(sooner) == expert_of(later)), 1.0, 0.0
+    ).astype(jnp.bfloat16)
+    before = dot(member.astype(jnp.bfloat16), earlier)
+    start = (group_lane * capacity).astype(jnp.float32)
+    info[0:eps, 0:wide] = jnp.where(member > 0.5, before + start, -1.0)
+    info_cols[...] = jnp.transpose(info[...])
+
+    def column(index):
+        lane = lax.broadcasted_iota(jnp.int32, (wide, info_cols.shape[1]), 1)
+        picked = jnp.where(lane == index, info_cols[0:wide, :], 0.0)
+        return jnp.sum(picked, 1, keepdims=True)
+
+    def groups(step):
+        return chip_at(step) * 2 + core, chip_at(step) * 2 + 1 - core
+
+    hidden_copies = {}
+    side_copies = {}
+    side_span = pl.ds(pl.multiple_of(ep * side_rows, side_rows), side_rows)
+
+    def expert_step(step):
+        for at, g in enumerate(groups(step)):
+            sums = jnp.zeros((rows, half), jnp.float32)
+            squares = jnp.zeros((rows, half), jnp.float32)
+            for part in range(2 * tps):
+                x = rows_all[g, part].astype(jnp.float32)
+                sums = sums + x
+                squares = squares + x * x
+            mean = jnp.sum(sums, 1, keepdims=True) / model
+            square = jnp.sum(squares, 1, keepdims=True) / model
+            scale = lax.rsqrt(square - mean * mean + NORM_EPS)
+            for part in range(2 * tps):
+                span = slice(part * half, (part + 1) * half)
+                x = rows_all[g, part].astype(jnp.float32)
+                y = ((x - mean) * scale * first_gain[:, span]).astype(jnp.bfloat16)
+                normed[at * rows : (at + 1) * rows, span] = y
+                if step == 0 and at == 0:
+                    own_normed[:, span] = y
+        if step == 0:
+            ready("side")
+        side_part = lax.dot_general(
+            normed[:, side_span],
+            side_w[...],
+            (((1,), (1,)), ((), ())),
+            preferred_element_type=jnp.float32,
+        ).astype(jnp.bfloat16)
+        side_copies[step] = []
+        for at, g in enumerate(groups(step)):
+            side_out[step, at] = side_part[at * rows : (at + 1) * rows]
+            if step > 0 or at > 0:
+                side_copies[step].append(
+                    push(side_out.at[step, at], side_in.at[step, at], side_sems, (step, at), (g, tp))
+                )
+        if step == 0:
+            ready("gate_up")
+        stacks = [[], []]
+        scales = [column(eps + g) for g in groups(step)]
+        for e in range(experts):
+            both = dot(normed[...], gate_up_w[e])
+            hidden = silu(both[:, :hidden_width]) * both[:, hidden_width:]
+            for at in range(2):
+                mine = hidden[at * rows : (at + 1) * rows] * scales[at][e * rows : (e + 1) * rows]
+                stacks[at].append(mine.astype(jnp.bfloat16))
+        for at, g in enumerate(groups(step)):
+            slot_row = info[pl.ds(g, 1), 0:wide]
+            number = lax.broadcasted_iota(jnp.int32, (slots, wide), 0).astype(jnp.float32)
+            table = jnp.where(number == slot_row, 1.0, 0.0).astype(jnp.bfloat16)
+            packed = dot(table, jnp.concatenate(stacks[at], 0)).astype(jnp.bfloat16)
+            hidden_all[step, tp, at] = packed
+        hidden_copies[step] = [
+            push(hidden_all.at[step, tp], hidden_all.at[step, tp], hidden_sems, (step, i), p)
+            for i, p in enumerate(plane)
+        ]
+
+    pair_copies = {}
+    line_copies = {}
+
+    def down_step(step):
+        for copy in hidden_copies[step]:
+            copy.wait_recv()
+        if step == 0:
+            ready("down")
+        spread_rows = []
+        for at, g in enumerate(groups(step)):
+            number = lax.broadcasted_iota(jnp.int32, (wide, slots), 1).astype(jnp.float32)
+            table = jnp.where(number == column(g), 1.0, 0.0).astype(jnp.bfloat16)
+            packed = jnp.concatenate([hidden_all[step, t, at] for t in range(tps)], 1)
+            spread_rows.append(dot(table, packed).astype(jnp.bfloat16))
+        result = None
+        for e in range(experts):
+            mine = jnp.concatenate([r[e * rows : (e + 1) * rows] for r in spread_rows], 0)
+            term = dot(mine, down_w[e])
+            result = term if result is None else result + term
+        total[step] = result[:rows]
+        pair_out[step] = result[rows:].astype(jnp.bfloat16)
+        pair_copies[step] = push(
+            pair_out.at[step], pair_in.at[step], back_sems, (step, 0), partner
+        )
+
+    def return_step(step):
+        pair_copies[step].wait_recv()
+        mine = total[step] + pair_in[step].astype(jnp.float32)
+        if step == 0:
+            total[step] = mine
+            return
+        line_out[step] = mine.astype(jnp.bfloat16)
+        line_copies[step] = push(
+            line_out.at[step],
+            line_in.at[step],
+            back_sems,
+            (step, 1),
+            (chip_at(step) * 2 + core, tp),
+        )
+
+    def own_shared():
+        ready("shared")
+        both = dot(own_normed[...], shared_w[...])
+        hidden = silu(both[:, :shared_width]) * both[:, shared_width:]
+        late_all[tp, :, 0:shared_width] = hidden.astype(jnp.bfloat16)
+
+    late_copies = []
+
+    def own_side():
+        pre = side_out[0, 0].astype(jnp.float32)
+        for step in range(steps):
+            for at, copy in enumerate(side_copies[step]):
+                place = at + 1 if step == 0 else at
+                copy.wait_recv()
+                pre = pre + side_in[step, place].astype(jnp.float32)
+        act = silu(pre[:, :side_width]) * pre[:, side_width:]
+        act = jnp.concatenate([act, jnp.zeros_like(act)], 1)
+        late_all[tp, :, shared_width : shared_width + 2 * side_width] = act.astype(jnp.bfloat16)
+        late_copies.extend(
+            push(late_all.at[tp], late_all.at[tp], late_sems, (i,), p) for i, p in enumerate(plane)
+        )
+
+    def own_extra():
+        product = own_normed[...].astype(jnp.float32) * side_switch[...].astype(jnp.float32)
+        logit = jnp.sum(product, 1, keepdims=True)
+        switch = 1.0 / (1.0 + jnp.exp(-logit))
+        ready("late")
+        for copy in late_copies:
+            copy.wait_recv()
+        shared = jnp.concatenate([late_all[t, :, :shared_width] for t in range(tps)], 1)
+        shared = dot(shared, shared_down_w[...])
+        side = None
+        for t in range(tps):
+            mine = late_all[t, :, shared_width : shared_width + side_width]
+            term = dot(mine, side_down_w[t * side_width : (t + 1) * side_width, :])
+            side = term if side is None else side + term
+        return shared + switch * side
+
+    relay(0)
+    corner(0)
+    spread(1)
+    arrive(0)
+    relay(1)
+    expert_step(0)
+    spread(2)
+    corner(1)
+    arrive(1)
+    relay(2)
+    expert_step(1)
+    spread(3)
+    corner(2)
+    arrive(2)
+    relay(3)
+    down_step(0)
+    expert_step(2)
+    corner(3)
+    arrive(3)
+    return_step(0)
+    expert_step(3)
+    down_step(1)
+    own_shared()
+    return_step(1)
+    down_step(2)
+    own_side()
+    return_step(2)
+    down_step(3)
+    extra = own_extra()
+    return_step(3)
+
+    routed = total[0]
+    for step in range(1, steps):
+        line_copies[step].wait_recv()
+        routed = routed + line_in[step].astype(jnp.float32)
+    own = own_normed[:, pl.ds(pl.multiple_of(tp * cols, cols), cols)].astype(jnp.float32)
+    pre_second = RESIDUAL_SCALE * own + routed + extra
+    lane = lax.broadcasted_iota(jnp.int32, (rows, stats.shape[2]), 1)
+    sums = jnp.sum(pre_second, 1, keepdims=True)
+    squares = jnp.sum(pre_second * pre_second, 1, keepdims=True)
+    stats[tp] = jnp.where(lane == 0, sums, squares)
+    stat_copies = [push(stats.at[tp], stats.at[tp], stat_sems, (i,), p) for i, p in enumerate(plane)]
+    for copy in stat_copies:
+        copy.wait_recv()
+    totals = stats[0]
+    for t in range(1, tps):
+        totals = totals + stats[t]
+    mean = jnp.sum(jnp.where(lane == 0, totals, 0.0), 1, keepdims=True) / model
+    square = jnp.sum(jnp.where(lane == 1, totals, 0.0), 1, keepdims=True) / model
+    scale = lax.rsqrt(square - mean * mean + NORM_EPS)
+    output[...] = ((pre_second - mean) * scale * second_gain[...]).astype(output.dtype)
+    for copy in pending:
+        copy.wait_send()
+
+
+def mixer(
+    mixed,
+    tokens,
+    routes,
+    route_weights,
+    first_gain,
+    second_gain,
+    side_switch,
+    weights,
+):
+    out_w, gate_w, up_w, down_w, shared_gate, shared_up, shared_down, side_gate, side_up, side_down = weights
+    eps, tps = lax.axis_size("ep"), lax.axis_size("tp")
+    chips = eps // 2
+    rows, model = tokens.shape
+    cols = model // tps
+    experts, _, hidden = gate_w.shape
+    top = routes.shape[0]
+    total = experts * eps
+    capacity = (3 * rows * top + total - 1) // total
+    slots = -(-experts * capacity // 16) * 16
+    wide = -(-experts * rows // 128) * 128
+    side_width, side_rows = side_gate.shape
+    shared = shared_gate.shape[1]
+    bf16, f32 = jnp.bfloat16, jnp.float32
+    dma = pltpu.SemaphoreType.DMA
+    return pl.pallas_call(
+        functools.partial(mixer_body, (chips, tps, capacity)),
+        out_shape=jax.ShapeDtypeStruct((rows, cols), bf16),
+        in_specs=[VMEM] * 7 + [ANY] * 10,
+        out_specs=VMEM,
+        scratch_shapes=[
+            pltpu.VMEM((tps,) + mixed.shape, bf16),
+            pltpu.VMEM((eps, top, rows), jnp.int32),
+            pltpu.VMEM((eps, top, rows), f32),
+            pltpu.VMEM((eps, 2 * tps, rows, cols // 2), bf16),
+            pltpu.VMEM((2 * rows, model), bf16),
+            pltpu.VMEM((rows, model), bf16),
+            pltpu.VMEM((128, wide), f32),
+            pltpu.VMEM((wide, 128), f32),
+            pltpu.VMEM((chips, tps, 2, slots, hidden), bf16),
+            pltpu.VMEM((chips, rows, cols), bf16),
+            pltpu.VMEM((chips, rows, cols), bf16),
+            pltpu.VMEM((chips, rows, cols), bf16),
+            pltpu.VMEM((chips, rows, cols), bf16),
+            pltpu.VMEM((chips, rows, cols), f32),
+            pltpu.VMEM((chips, 2, rows, 2 * side_width), bf16),
+            pltpu.VMEM((chips, 2, rows, 2 * side_width), bf16),
+            pltpu.VMEM((tps, rows, shared + 2 * side_width), bf16),
+            pltpu.VMEM((tps, rows, 128), f32),
+            pltpu.VMEM(out_w.shape, bf16),
+            pltpu.VMEM((experts, model, 2 * hidden), bf16),
+            pltpu.VMEM(down_w.shape, bf16),
+            pltpu.VMEM((model, 2 * shared), bf16),
+            pltpu.VMEM(shared_down.shape, bf16),
+            pltpu.VMEM((2 * side_width, side_rows), bf16),
+            pltpu.VMEM(side_down.shape, bf16),
+            dma((2 * experts + 8,)),
+            dma((2, tps - 1)),
+            dma((2, eps - 1, 2)),
+            dma((2, chips, 10)),
+            dma((2, chips, tps - 1)),
+            dma((2, chips, 2)),
+            dma((2, chips, 2)),
+            dma((2, tps - 1)),
+            dma((2, tps - 1)),
+        ],
+        compiler_params=pltpu.CompilerParams(collective_id=0, has_side_effects=True),
+    )(mixed, tokens, routes, route_weights, first_gain, second_gain, side_switch, *weights)
+
+
+def streamed_device(
+    tokens,
+    retention_state,
+    lengths,
+    query_weight,
+    key_weight,
+    value_weight,
+    gate_weight,
+    out_weight,
+    first_gain,
+    routing,
+    route_weight,
+    expert_gate,
+    expert_up,
+    expert_down,
+    shared_gate,
+    shared_up,
+    shared_down,
+    side_gate,
+    side_up,
+    side_down,
+    side_switch,
+    second_gain,
+):
+    rows, heads, width = retention_state.shape[:3]
+    exponent = np.arange(width // 2, dtype=np.float64) / (width // 2)
+    frequency = np.tile((ROPE_BASE**-exponent).astype(np.float32), 2 * heads)[None, :]
+    mixed, new_state = retain_kernel(
+        tokens,
+        lengths.reshape(1, rows),
+        jnp.asarray(frequency),
+        [query_weight, key_weight, value_weight, gate_weight],
+        retention_state,
+    )
+    output = mixer(
+        mixed,
+        tokens,
+        routing.T,
+        route_weight.T,
+        first_gain.reshape(1, -1),
+        second_gain.reshape(1, -1),
+        side_switch.reshape(1, -1),
+        [
+            out_weight,
+            expert_gate,
+            expert_up,
+            expert_down,
+            shared_gate,
+            shared_up,
+            shared_down,
+            side_gate.T,
+            side_up.T,
+            side_down,
+        ],
+    )
+    return (output, new_state)
+
+
+def staged_device(
     tokens,
     retention_state,
     lengths,
@@ -489,6 +1191,23 @@
     return (output, new_state)
 
 
+def on_device(*arrays):
+    tokens, state, expert_gate, side_gate = arrays[0], arrays[1], arrays[11], arrays[17]
+    eps, tps = lax.axis_size("ep"), lax.axis_size("tp")
+    rows, model = tokens.shape
+    fits = (
+        eps == 8
+        and tps == 4
+        and rows % 16 == 0
+        and model % (256 * tps) == 0
+        and state.shape[1] * state.shape[2] % 128 == 0
+        and expert_gate.shape[2] % 128 == 0
+        and side_gate.shape[0] % 128 == 0
+        and side_gate.shape[1] == 64
+    )
+    return (streamed_device if fits else staged_device)(*arrays)
+
+
 def solution(mesh):
     return jax.shard_map(
         on_device,

time: 125 us -> 66.8 us (0.53)
  other arithmetic: 22.4 us -> 0 us
  Pallas kernels: 76.2 us -> 63.2 us
  matrix products: 11.8 us -> 0 us
  local copies, waits for them, and re-layouts: 12.2 us -> 2.71 us
    pallas_call x7 -> x2, Pallas kernels: 76.2 us -> 63.2 us  [the longest x1 52.3 us: mixer(): pl.pallas_call(functools.partial(mixer_body, (chips, tps, capacity)), out...]
    dot_general x11 -> x0, matrix products: 11.8 us -> none  [the longest x1 1.75 us: on_device(): jnp.dot(normed_full, shared_up, preferred_element_type=jnp.float32)]
    add x2 -> x0, other arithmetic: 9.17 us -> none  [the longest x1 9.16 us: retain(): decays[None, :, None, None] * retention_state]
    convert_element_type x6 -> x0, other arithmetic: 5.02 us -> none  [the longest x1 1.44 us: retain(): mixed_heads = (normed.reshape(row_count, head_count * head_width) * jax.n...]
    reduce_sum x8 -> x0, other arithmetic: 4.89 us -> none  [the longest x2 1.4 us: row_moments(): totals = jnp.sum(every, 0)]
    mul x6 -> x0, local copies, waits for them, and re-layouts: 1.78 us -> none  [the longest x2 0.85 us: retain(): own_term = jnp.sum(queries * key_rows, -1, keepdims=True) * values]
    transpose x2 -> x0, local copies, waits for them, and re-layouts: 1.45 us -> none  [the longest x1 0.73 us: on_device(): jnp.transpose(every_weight, (1, 0, 2)).reshape(top_count, total_rows)]
    unnamed x40 -> x1, local copies, waits for them, and re-layouts: 2.83 us -> 1.42 us
where the time goes in v1:
time: 66.8 us; the launch traced here: 66.6 us
  Pallas kernels  63.2 us (95%)
  local copies, waits for them, and re-layouts  2.71 us (4%)
    pallas_call x1, Pallas kernels, mixer(): pl.pallas_call(functools.partial(mixer_body, (chips, tps, capacity)), out...  52.3 us
    pallas_call x1, Pallas kernels, retain_kernel(): pl.pallas_call(functools.partial(retain_body, chunk), out_shape=[jax.Shap...  10.9 us
    unnamed x1, local copies, waits for them, and re-layouts  1.42 us

profile of v1, /device:TPU:0, one launch (start us, length us, event | category | flops | bytes accessed | tf_op | source)
XLA Modules:
  0.0 66.6 jit_solution(9793323419542463631)
XLA Ops:
  0.6 1.3 %reshape.19.side_switch = bf16[1,2048]{1,0:T(2,128)(2,1)} reshape(bf16[2048]{0:T(1024)(128)(2,1)} %param.43) | data formatting | bytes 8192 | tf_op jit(solution)/shard_map/reshape | solution.py:1031
  1.9 10.9 %shard_map.230 = (bf16[48,256]{1,0:T(8,128)(2,1)}, f32[48,4,64,64]{3,2,1,0:T(8,128)}) custom-call(bf16[48,2048]{1,0:T(8,128)(2,1)} %tokens.1, s32[1,48]{1,0:T(1,128)} %bitcast.13, f32[1,256]{1,0:T(1,128)} %constant.2.clone.frequency, bf16[2048,256]{1,0:T(8,128)(2,1)} %query_in.1, bf16[2048,256]{1,0:T(8,128)(2,1)} %key_in.1, bf16[2048,256]{1,0:T(8,128)(2,1)} %value_in.1, ...), custom_call_target="tpu_custom_call" | custom-call | tf_op jit(solution)/shard_map/pallas_call | solution.py:474
  12.8 52.3 %shard_map.231 = bf16[48,512]{1,0:T(8,128)(2,1)} custom-call(bf16[48,256]{1,0:T(8,128)(2,1)} %get-tuple-element.4.mixed, bf16[48,2048]{1,0:T(8,128)(2,1)} %tokens.1, s32[4,48]{1,0:T(4,128)} %bitcast.10, f32[4,48]{1,0:T(4,128)} %bitcast.11, f32[1,2048]{1,0:T(1,128)} %bitcast.9, f32[1,512]{1,0:T(1,128)} %bitcast.12, bf16[1,2048]{1,0:T(2,128)(2,1)} %reshape.19.side_switch, ...), custom_call_target="tpu_custom_call" | custom-call | tf_op jit(solution)/shard_map/pallas_call | solution.py:945
  65.2 1.4 %copy.26 = bf16[48,512]{1,0:T(8,128)(2,1)} copy(bf16[48,512]{1,0:T(8,128)(2,1)} %shard_map.231) | data formatting | bytes 98304

commit v2 on v0

--- a/solution.py
+++ b/solution.py
@@ -2,6 +2,7 @@
 
 import jax
 import jax.numpy as jnp
+import numpy as np
 from jax import lax
 from jax.experimental import pallas as pl
 from jax.experimental.pallas import tpu as pltpu
@@ -343,7 +344,805 @@
     return totals[0][:, None], totals[1][:, None]
 
 
-def on_device(
+ANY = pl.BlockSpec(memory_space=pl.ANY)
+
+
+def dot(a, b):
+    return jnp.dot(a, b, preferred_element_type=jnp.float32)
+
+
+def silu(x):
+    return x / (1.0 + jnp.exp(-x))
+
+
+def fetch(source, target, sem):
+    copy = pltpu.make_async_copy(source, target, sem)
+    copy.start()
+    return copy
+
+
+def settle(ref, sem):
+    pltpu.make_async_copy(ref, ref, sem).wait()
+
+
+def on_diagonal(rows):
+    row = lax.broadcasted_iota(jnp.int32, (rows, rows), 0)
+    return row == lax.broadcasted_iota(jnp.int32, (rows, rows), 1)
+
+
+def column_of(line):
+    return jnp.sum(jnp.where(on_diagonal(line.shape[1]), line, 0.0), 1, keepdims=True)
+
+
+def line_of(column):
+    return jnp.sum(jnp.where(on_diagonal(column.shape[0]), column, 0.0), 0, keepdims=True)
+
+
+def rotated(x, cosine, sine, half):
+    width = x.shape[1]
+    lane = lax.broadcasted_iota(jnp.int32, x.shape, 1)
+    first = (lane & (2 * half - 1)) < half
+    later = pltpu.roll(x, width - half, 1)
+    sooner = pltpu.roll(x, half, 1)
+    return x * cosine + jnp.where(first, -later, sooner) * sine
+
+
+def retain_body(
+    chunk,
+    tokens_in,
+    lengths_in,
+    frequency_in,
+    query_in,
+    key_in,
+    value_in,
+    gate_in,
+    state_in,
+    mixed,
+    state_out,
+    tokens,
+    lengths,
+    frequency,
+    weights,
+    state,
+    columns,
+    spread_even,
+    spread_odd,
+    values,
+    carried,
+    small_sem,
+    weight_sem,
+    state_sem,
+    out_sem,
+):
+    rows, heads, width = state.shape[0], state.shape[1], state.shape[2]
+    total = heads * width
+    chunks = rows // chunk
+    small = [
+        fetch(source, target, small_sem.at[i])
+        for i, (source, target) in enumerate(
+            [(lengths_in, lengths), (frequency_in, frequency), (tokens_in, tokens)]
+        )
+    ]
+    for i, source in enumerate([query_in, key_in, value_in, gate_in]):
+        fetch(source, weights.at[:, pl.ds(i * total, total)], weight_sem.at[i // 2])
+    for i in range(chunks):
+        piece = pl.ds(i * chunk, chunk)
+        fetch(state_in.at[piece], state.at[piece], state_sem.at[i])
+
+    with jax.named_scope("small_wait"):
+        small[0].wait()
+        small[1].wait()
+    position = column_of(lengths[...].astype(jnp.float32))
+    angles = position * frequency[...]
+    cosine, sine = jnp.cos(angles), jnp.sin(angles)
+    first_head = lax.axis_index("tp") * heads
+    decays = []
+    for head in range(heads):
+        index = jnp.full((1, width), first_head + head, jnp.int32).astype(jnp.float32)
+        decays.append(1.0 - jnp.exp2(-5.0 - 7.0 * index / (HEADS - 1)))
+
+    def project(i):
+        span = pl.ds(2 * i * total, 2 * total)
+        with jax.named_scope("weight_wait"):
+            settle(weights.at[:, span], weight_sem.at[i])
+        both = dot(tokens[...], weights[:, span]).astype(jnp.bfloat16).astype(jnp.float32)
+        return both[:, :total], both[:, total:]
+
+    with jax.named_scope("small_wait"):
+        small[2].wait()
+    query, key = project(0)
+    lanes = columns.shape[1] // 2
+    for i, (x, scale) in enumerate([(query, 1.0), (key, width ** (-0.5))]):
+        turned = rotated(x, cosine, sine, width // 2) * scale
+        padded = jnp.concatenate([turned, jnp.zeros((lanes - rows, total), jnp.float32)], 0)
+        flipped = jnp.transpose(padded)
+        high = flipped.astype(jnp.bfloat16)
+        columns[i * total : (i + 1) * total, :lanes] = high
+        columns[i * total : (i + 1) * total, lanes:] = (
+            flipped - high.astype(jnp.float32)
+        ).astype(jnp.bfloat16)
+    value, gate = project(1)
+    for head in range(heads):
+        values[head] = value[:, head * width : (head + 1) * width]
+
+    source_lane = lax.broadcasted_iota(jnp.int32, (2 * lanes, 2 * lanes), 0) & (lanes - 1)
+    target_lane = lax.broadcasted_iota(jnp.int32, (2 * lanes, 2 * lanes), 1)
+    offset = jnp.where(target_lane >= lanes, 1, 0)
+    buffers = [spread_even, spread_odd]
+
+    def widen(i):
+        for pair in range(chunk // 2):
+            pick = jnp.where(source_lane == offset + (i * chunk + 2 * pair), 1.0, 0.0)
+            buffers[i % 2][pair] = dot(columns[...], pick.astype(jnp.bfloat16))
+
+    widen(0)
+    for i in range(chunks):
+        base = i * chunk
+        piece = pl.ds(base, chunk)
+        with jax.named_scope("state_wait"):
+            pltpu.make_async_copy(state_in.at[piece], state.at[piece], state_sem.at[i]).wait()
+        if i + 1 < chunks:
+            widen(i + 1)
+        wide = buffers[i % 2]
+        for at in range(chunk):
+            lane = (at % 2) * lanes
+            for head in range(heads):
+                low, high = head * width, (head + 1) * width
+                q_cols = wide[at // 2, low:high, lane : lane + width]
+                k_cols = wide[at // 2, total + low : total + high, lane : lane + width]
+                v_row = values[head, base + at : base + at + 1, :]
+                new = decays[head] * state[base + at, head] + k_cols * v_row
+                state[base + at, head] = new
+                carried[head, base + at : base + at + 1, :] = jnp.sum(
+                    q_cols * new, 0, keepdims=True
+                )
+        fetch(state.at[piece], state_out.at[piece], out_sem)
+    parts = []
+    for head in range(heads):
+        result = carried[head]
+        scale = lax.rsqrt(jnp.mean(result * result, -1, keepdims=True) + GROUP_EPS)
+        parts.append(result * scale)
+    mixed[...] = (jnp.concatenate(parts, 1) * silu(gate)).astype(mixed.dtype)
+    with jax.named_scope("state_drain"):
+        settle(state, out_sem)
+
+
+def retain_kernel(tokens, lengths, frequency, weights, state):
+    rows, heads, width = state.shape[0], state.shape[1], state.shape[2]
+    chunk, lanes = 8, 128
+    cols = heads * width
+    wide = pltpu.VMEM((chunk // 2, 2 * cols, 2 * lanes), jnp.float32)
+    return pl.pallas_call(
+        functools.partial(retain_body, chunk),
+        out_shape=[
+            jax.ShapeDtypeStruct((rows, cols), jnp.bfloat16),
+            jax.ShapeDtypeStruct(state.shape, state.dtype),
+        ],
+        in_specs=[ANY] * 8,
+        out_specs=[VMEM, ANY],
+        scratch_shapes=[
+            pltpu.VMEM(tokens.shape, tokens.dtype),
+            pltpu.VMEM(lengths.shape, lengths.dtype),
+            pltpu.VMEM(frequency.shape, frequency.dtype),
+            pltpu.VMEM((tokens.shape[1], 4 * cols), jnp.bfloat16),
+            pltpu.VMEM(state.shape, state.dtype),
+            pltpu.VMEM((2 * cols, 2 * lanes), jnp.bfloat16),
+            wide,
+            wide,
+            pltpu.VMEM((heads, rows, width), jnp.float32),
+            pltpu.VMEM((heads, rows, width), jnp.float32),
+            pltpu.SemaphoreType.DMA((3,)),
+            pltpu.SemaphoreType.DMA((2,)),
+            pltpu.SemaphoreType.DMA((rows // chunk,)),
+            pltpu.SemaphoreType.DMA,
+        ],
+    )(tokens, lengths, frequency, *weights, state)
+
+
+def mixer_body(
+    dims,
+    mixed_in,
+    tokens_in,
+    routes_in,
+    route_weights_in,
+    first_gain_in,
+    side_switch_in,
+    out_in,
+    gate_in,
+    up_in,
+    down_in,
+    shared_gate_in,
+    shared_up_in,
+    shared_down_in,
+    side_gate_in,
+    side_up_in,
+    side_down_in,
+    output,
+    own_tokens,
+    first_gain,
+    side_switch,
+    mixed_all,
+    route_all,
+    weight_all,
+    rows_all,
+    normed,
+    info,
+    info_cols,
+    hidden_all,
+    pair_out,
+    pair_in,
+    line_out,
+    line_in,
+    total,
+    side_out,
+    side_in,
+    late_all,
+    stats,
+    out_w,
+    gate_up_w,
+    down_w,
+    shared_w,
+    shared_down_w,
+    side_w,
+    side_down_w,
+    small_sem,
+    weight_sem,
+    send_sem,
+    recv_sem,
+    row_sem,
+    back_sem,
+):
+    chips, tps, capacity = dims
+    steps = chips
+    rows, cols = own_tokens.shape
+    model = cols * tps
+    half = cols // 2
+    experts, hidden_width = gate_in.shape[0], gate_in.shape[2]
+    slots = hidden_all.shape[3]
+    side_width = side_gate_in.shape[0]
+    side_rows = side_gate_in.shape[1]
+    shared_width = shared_gate_in.shape[1]
+    tp = lax.axis_index("tp")
+    ep = lax.axis_index("ep")
+    eps = 2 * chips
+    chip, core = ep // 2, lax.rem(ep, 2)
+    partner = (chip * 2 + 1 - core, tp)
+    low, high = lax.rem(tp, 2), tp // 2
+    tp_x = high * 2 + 1 - low
+    tp_y = (1 - high) * 2 + low
+    tp_d = (1 - high) * 2 + 1 - low
+    plane = [(ep, tp_x), (ep, tp_y), (ep, tp_d)]
+
+    def chip_at(step):
+        if step == 0:
+            return chip
+        if step == 1:
+            return chip + 1 - 2 * lax.rem(chip, 2)
+        if step == 2:
+            return lax.rem(chip + 2, 4)
+        return 3 - chip
+
+    def group_at(step, at):
+        return chip_at(step) * 2 + (core if at == 0 else 1 - core)
+
+    line = [(group_at(step, 0), tp) for step in range(steps)]
+    others = [(group_at(s, at), tp) for s in range(steps) for at in range(2) if s + at > 0]
+    peers = plane + others
+    barrier = pltpu.get_barrier_semaphore()
+    for peer in peers:
+        pl.semaphore_signal(barrier, inc=1, device_id=peer, device_id_type=DEVICE)
+
+    own_mixed = mixed_all.at[tp]
+    own_slice = pl.ds(pl.multiple_of(tp * cols, cols), cols)
+    fetch(mixed_in, own_mixed, small_sem.at[0])
+    fetch(routes_in, route_all.at[ep], small_sem.at[1])
+    fetch(route_weights_in, weight_all.at[ep], small_sem.at[2])
+    fetch(tokens_in.at[:, own_slice], own_tokens, small_sem.at[3])
+    fetch(out_in, out_w, weight_sem.at[0])
+    fetch(first_gain_in, first_gain, small_sem.at[4])
+    fetch(side_switch_in, side_switch, small_sem.at[5])
+    for e in range(experts):
+        fetch(gate_in.at[e], gate_up_w.at[e, :, pl.ds(0, hidden_width)], weight_sem.at[1])
+        fetch(up_in.at[e], gate_up_w.at[e, :, pl.ds(hidden_width, hidden_width)], weight_sem.at[1])
+    fetch(side_gate_in, side_w.at[pl.ds(0, side_width)], weight_sem.at[2])
+    fetch(side_up_in, side_w.at[pl.ds(side_width, side_width)], weight_sem.at[2])
+    fetch(shared_gate_in, shared_w.at[:, pl.ds(0, shared_width)], weight_sem.at[3])
+    fetch(shared_up_in, shared_w.at[:, pl.ds(shared_width, shared_width)], weight_sem.at[3])
+    fetch(down_in, down_w, weight_sem.at[4])
+    fetch(shared_down_in, shared_down_w, weight_sem.at[5])
+    fetch(side_down_in, side_down_w, weight_sem.at[6])
+
+    MIXED, ROUTE, WEIGHT, SIDE, LATE, STAT, HIDDEN = 0, 1, 2, 3, 4, 5, 6
+
+    def push(source, target, sent, received, peer):
+        send(source, target, sent, received, peer)
+
+    with jax.named_scope("small_wait"):
+        settle(own_mixed, small_sem.at[0])
+        settle(route_all.at[ep], small_sem.at[1])
+        settle(weight_all.at[ep], small_sem.at[2])
+    with jax.named_scope("enter"):
+        pl.semaphore_wait(barrier, len(peers))
+
+    for peer in plane:
+        push(own_mixed, own_mixed, send_sem.at[MIXED], recv_sem.at[MIXED], peer)
+    for peer in others:
+        own = route_all.at[ep]
+        push(own, own, send_sem.at[ROUTE], recv_sem.at[ROUTE], peer)
+        own = weight_all.at[ep]
+        push(own, own, send_sem.at[WEIGHT], recv_sem.at[WEIGHT], peer)
+
+    with jax.named_scope("out_wait"):
+        settle(own_tokens, small_sem.at[3])
+        settle(out_w, weight_sem.at[0])
+    with jax.named_scope("mixed_wait"):
+        settle(mixed_all.at[pl.ds(0, tps - 1)], recv_sem.at[MIXED])
+    heads_all = jnp.concatenate([mixed_all[t] for t in range(tps)], 1)
+    pre_first = RESIDUAL_SCALE * own_tokens[...].astype(jnp.float32) + dot(heads_all, out_w[...])
+    for part in range(2):
+        rows_all[ep, 2 * tp + part] = pre_first[:, part * half : (part + 1) * half].astype(
+            jnp.bfloat16
+        )
+
+    def block(step, index):
+        return rows_all.at[group_at(step, 0), pl.ds(2 * index, 2)]
+
+    def piece(step, index, part):
+        return rows_all.at[group_at(step, 0), 2 * index + part]
+
+    def push_rows(ref, step, kind, peer):
+        sent = send_sem.at[8] if kind == 5 else send_sem.at[7]
+        push(ref, ref, sent, row_sem.at[step, kind], peer)
+
+    def came(ref, step, kind):
+        settle(ref, row_sem.at[step, kind])
+
+    def spread(step):
+        ref = block(step, tp)
+        if step > 0:
+            came(ref, step, 0)
+        push_rows(ref, step, 1, plane[0])
+        push_rows(ref, step, 2, plane[1])
+        push_rows(ref, step, 5, partner)
+
+    def relay(step):
+        came(block(step, tp_x), step, 1)
+        push_rows(piece(step, tp_x, 0), step, 3, plane[1])
+        push_rows(block(step, tp_x), step, 5, partner)
+        came(block(step, tp_y), step, 2)
+        push_rows(piece(step, tp_y, 1), step, 4, plane[0])
+        push_rows(block(step, tp_y), step, 5, partner)
+
+    def corner(step):
+        for part in range(2):
+            came(piece(step, tp_d, part), step, 3 + part)
+            push_rows(piece(step, tp_d, part), step, 5, partner)
+
+    def arrive(step):
+        came(rows_all.at[group_at(step, 1)], step, 5)
+
+    with jax.named_scope("spread0"):
+        spread(0)
+        for step in range(1, steps):
+            push_rows_to = line[step]
+            push(block(0, tp), block(0, tp), send_sem.at[7], row_sem.at[step, 0], push_rows_to)
+
+    with jax.named_scope("route_wait"):
+        settle(route_all.at[pl.ds(0, eps - 1)], recv_sem.at[ROUTE])
+        settle(weight_all.at[pl.ds(0, eps - 1)], recv_sem.at[WEIGHT])
+    wide = experts * rows
+
+    def expert_of(index):
+        return sum(jnp.where(index >= e * rows, 1, 0) for e in range(1, experts))
+
+    group_lane = expert_of(lax.broadcasted_iota(jnp.int32, (1, wide), 1))
+    expert_lane = ep * experts + group_lane
+    info[...] = jnp.zeros_like(info)
+    for g in range(eps):
+        ids = jnp.concatenate([route_all[g]] * experts, 1)
+        hits = ids == expert_lane
+        scales = jnp.concatenate([weight_all[g]] * experts, 1)
+        info[g : g + 1, 0:wide] = jnp.sum(jnp.where(hits, 1.0, 0.0), 0, keepdims=True)
+        info[eps + g : eps + g + 1, 0:wide] = jnp.sum(
+            jnp.where(hits, scales, 0.0), 0, keepdims=True
+        )
+    member = info[0:eps, 0:wide]
+    sooner = lax.broadcasted_iota(jnp.int32, (wide, wide), 0)
+    later = lax.broadcasted_iota(jnp.int32, (wide, wide), 1)
+    earlier = jnp.where(
+        (sooner < later) & (expert_of(sooner) == expert_of(later)), 1.0, 0.0
+    ).astype(jnp.bfloat16)
+    before = dot(member.astype(jnp.bfloat16), earlier)
+    start = (group_lane * capacity).astype(jnp.float32)
+    info[0:eps, 0:wide] = jnp.where(member > 0.5, before + start, -1.0)
+    info_cols[...] = jnp.transpose(info[...])
+    settle(first_gain, small_sem.at[4])
+
+    def column(index):
+        lane = lax.broadcasted_iota(jnp.int32, (wide, info_cols.shape[1]), 1)
+        picked = jnp.where(lane == index, info_cols[0:wide, :], 0.0)
+        return jnp.sum(picked, 1, keepdims=True)
+
+    side_span = pl.ds(pl.multiple_of(ep * side_rows, side_rows), side_rows)
+
+    def blocks(group):
+        return [(step, at) for step in (2 * group, 2 * group + 1) for at in range(2)]
+
+    def norm_step(step, at):
+        g, base = group_at(step, at), (2 * step + at) * rows
+        sums = jnp.zeros((rows, half), jnp.float32)
+        squares = jnp.zeros((rows, half), jnp.float32)
+        for part in range(2 * tps):
+            x = rows_all[g, part].astype(jnp.float32)
+            sums = sums + x
+            squares = squares + x * x
+        mean = jnp.sum(sums, 1, keepdims=True) / model
+        square = jnp.sum(squares, 1, keepdims=True) / model
+        scale = lax.rsqrt(square - mean * mean + NORM_EPS)
+        for part in range(2 * tps):
+            span = slice(part * half, (part + 1) * half)
+            x = rows_all[g, part].astype(jnp.float32)
+            y = (x - mean) * scale * first_gain[:, span]
+            normed[base : base + rows, span] = y.astype(jnp.bfloat16)
+
+    def side_step(group):
+        if group == 0:
+            settle(side_w, weight_sem.at[2])
+        first = 4 * group * rows
+        partial = lax.dot_general(
+            normed[first : first + 4 * rows, side_span],
+            side_w[...],
+            (((1,), (1,)), ((), ())),
+            preferred_element_type=jnp.float32,
+        ).astype(jnp.bfloat16)
+        for i, (step, at) in enumerate(blocks(group)):
+            n = 2 * step + at
+            side_out[n] = partial[i * rows : (i + 1) * rows]
+            if n > 0:
+                peer = (group_at(step, at), tp)
+                push(
+                    side_out.at[n],
+                    side_in.at[n],
+                    send_sem.at[SIDE],
+                    recv_sem.at[SIDE],
+                    peer,
+                )
+
+    def expert_step(group):
+        if group == 0:
+            settle(gate_up_w, weight_sem.at[1])
+        first = 4 * group * rows
+        stacks = [[] for _ in range(4)]
+        scales = [column(eps + group_at(step, at)) for step, at in blocks(group)]
+        for e in range(experts):
+            both = dot(normed[first : first + 4 * rows, :], gate_up_w[e])
+            hidden = silu(both[:, :hidden_width]) * both[:, hidden_width:]
+            for i in range(4):
+                mine = hidden[i * rows : (i + 1) * rows] * scales[i][e * rows : (e + 1) * rows]
+                stacks[i].append(mine.astype(jnp.bfloat16))
+        for i, (step, at) in enumerate(blocks(group)):
+            slot_row = info[pl.ds(group_at(step, at), 1), 0:wide]
+            number = lax.broadcasted_iota(jnp.int32, (slots, wide), 0).astype(jnp.float32)
+            table = jnp.where(number == slot_row, 1.0, 0.0).astype(jnp.bfloat16)
+            packed = dot(table, jnp.concatenate(stacks[i], 0)).astype(jnp.bfloat16)
+            hidden_all[group, tp, i] = packed
+        own = hidden_all.at[group, tp]
+        for peer in plane:
+            push(own, own, send_sem.at[HIDDEN], recv_sem.at[HIDDEN + group], peer)
+
+    def down_step(group):
+        with jax.named_scope("hidden_wait"):
+            settle(hidden_all.at[group, pl.ds(0, tps - 1)], recv_sem.at[HIDDEN + group])
+        if group == 0:
+            settle(down_w, weight_sem.at[4])
+        spread_rows = []
+        for i, (step, at) in enumerate(blocks(group)):
+            number = lax.broadcasted_iota(jnp.int32, (wide, slots), 1).astype(jnp.float32)
+            table = jnp.where(number == column(group_at(step, at)), 1.0, 0.0).astype(jnp.bfloat16)
+            packed = jnp.concatenate([hidden_all[group, t, i] for t in range(tps)], 1)
+            spread_rows.append(dot(table, packed).astype(jnp.bfloat16))
+        result = None
+        for e in range(experts):
+            mine = jnp.concatenate([r[e * rows : (e + 1) * rows] for r in spread_rows], 0)
+            term = dot(mine, down_w[e])
+            result = term if result is None else result + term
+        for i, (step, at) in enumerate(blocks(group)):
+            part = result[i * rows : (i + 1) * rows]
+            if at == 0:
+                total[step] = part
+            else:
+                pair_out[step] = part.astype(jnp.bfloat16)
+        both = pl.ds(2 * group, 2)
+        push(
+            pair_out.at[both],
+            pair_in.at[both],
+            send_sem.at[9],
+            back_sem.at[group],
+            partner,
+        )
+
+    def return_step(group):
+        both = pl.ds(2 * group, 2)
+        with jax.named_scope("pair_wait"):
+            settle(pair_in.at[both], back_sem.at[group])
+        for step in (2 * group, 2 * group + 1):
+            mine = total[step] + pair_in[step].astype(jnp.float32)
+            if step == 0:
+                total[step] = mine
+                continue
+            line_out[step] = mine.astype(jnp.bfloat16)
+            push(
+                line_out.at[step],
+                line_in.at[step],
+                send_sem.at[10],
+                back_sem.at[1 + step],
+                line[step],
+            )
+
+    def own_shared():
+        settle(shared_w, weight_sem.at[3])
+        both = dot(normed[0:rows, :], shared_w[...])
+        hidden = silu(both[:, :shared_width]) * both[:, shared_width:]
+        late_all[tp, :, 0:shared_width] = hidden.astype(jnp.bfloat16)
+
+    def own_side():
+        with jax.named_scope("side_wait"):
+            settle(side_in.at[pl.ds(0, eps - 1)], recv_sem.at[SIDE])
+        pre = side_out[0].astype(jnp.float32)
+        for n in range(1, eps):
+            pre = pre + side_in[n].astype(jnp.float32)
+        act = silu(pre[:, :side_width]) * pre[:, side_width:]
+        act = jnp.concatenate([act, jnp.zeros_like(act)], 1)
+        late_all[tp, :, shared_width : shared_width + 2 * side_width] = act.astype(jnp.bfloat16)
+        for peer in plane:
+            push(late_all.at[tp], late_all.at[tp], send_sem.at[LATE], recv_sem.at[LATE], peer)
+
+    def own_switch():
+        settle(side_switch, small_sem.at[5])
+        row = side_switch[...].astype(jnp.float32)
+        product = normed[0:rows, :].astype(jnp.float32) * row
+        logit = jnp.sum(product, 1, keepdims=True)
+        return 1.0 / (1.0 + jnp.exp(-logit))
+
+    def own_extra():
+        settle(shared_down_w, weight_sem.at[5])
+        settle(side_down_w, weight_sem.at[6])
+        with jax.named_scope("late_wait"):
+            settle(late_all.at[pl.ds(0, tps - 1)], recv_sem.at[LATE])
+        shared = jnp.concatenate([late_all[t, :, :shared_width] for t in range(tps)], 1)
+        shared = dot(shared, shared_down_w[...])
+        side = None
+        for t in range(tps):
+            mine = late_all[t, :, shared_width : shared_width + side_width]
+            term = dot(mine, side_down_w[t * side_width : (t + 1) * side_width, :])
+            side = term if side is None else side + term
+        return shared + switch * side
+
+    with jax.named_scope("relay0"):
+        relay(0)
+    with jax.named_scope("spread1"):
+        spread(1)
+    with jax.named_scope("spread2"):
+        spread(2)
+    with jax.named_scope("corner0"):
+        corner(0)
+    with jax.named_scope("relay1"):
+        relay(1)
+    with jax.named_scope("spread3"):
+        spread(3)
+    with jax.named_scope("arrive0"):
+        arrive(0)
+    with jax.named_scope("norm_step0_0"):
+        norm_step(0, 0)
+    with jax.named_scope("norm_step0_1"):
+        norm_step(0, 1)
+    with jax.named_scope("relay2"):
+        relay(2)
+    with jax.named_scope("corner1"):
+        corner(1)
+    with jax.named_scope("relay3"):
+        relay(3)
+    with jax.named_scope("arrive1"):
+        arrive(1)
+    with jax.named_scope("norm_step1_0"):
+        norm_step(1, 0)
+    with jax.named_scope("norm_step1_1"):
+        norm_step(1, 1)
+    with jax.named_scope("side_step0"):
+        side_step(0)
+    with jax.named_scope("expert_step0"):
+        expert_step(0)
+    with jax.named_scope("corner2"):
+        corner(2)
+    with jax.named_scope("corner3"):
+        corner(3)
+    with jax.named_scope("arrive2"):
+        arrive(2)
+    with jax.named_scope("norm_step2_0"):
+        norm_step(2, 0)
+    with jax.named_scope("norm_step2_1"):
+        norm_step(2, 1)
+    with jax.named_scope("own_shared"):
+        own_shared()
+    with jax.named_scope("arrive3"):
+        arrive(3)
+    with jax.named_scope("norm_step3_0"):
+        norm_step(3, 0)
+    with jax.named_scope("norm_step3_1"):
+        norm_step(3, 1)
+    with jax.named_scope("side_step1"):
+        side_step(1)
+    with jax.named_scope("expert_step1"):
+        expert_step(1)
+    with jax.named_scope("down_step0"):
+        down_step(0)
+    with jax.named_scope("return_step0"):
+        return_step(0)
+    with jax.named_scope("own_switch"):
+        switch = own_switch()
+    with jax.named_scope("own_side"):
+        own_side()
+    with jax.named_scope("down_step1"):
+        down_step(1)
+    with jax.named_scope("own_extra"):
+        extra = own_extra()
+    with jax.named_scope("return_step1"):
+        return_step(1)
+
+    routed = total[0]
+    for step in range(1, steps):
+        with jax.named_scope("line_wait"):
+            settle(line_in.at[step], back_sem.at[1 + step])
+        routed = routed + line_in[step].astype(jnp.float32)
+    own = normed[0:rows, own_slice].astype(jnp.float32)
+    pre_second = RESIDUAL_SCALE * own + routed + extra
+    stats[tp, 0:1, 0:rows] = line_of(jnp.sum(pre_second, 1, keepdims=True))
+    stats[tp, 1:2, 0:rows] = line_of(jnp.sum(pre_second * pre_second, 1, keepdims=True))
+    for peer in plane:
+        push(stats.at[tp], stats.at[tp], send_sem.at[STAT], recv_sem.at[STAT], peer)
+    with jax.named_scope("stat_wait"):
+        settle(stats.at[pl.ds(0, tps - 1)], recv_sem.at[STAT])
+    totals = stats[0]
+    for t in range(1, tps):
+        totals = totals + stats[t]
+    mean = column_of(totals[0:1, 0:rows]) / model
+    square = column_of(totals[1:2, 0:rows]) / model
+    output[...] = (pre_second - mean) * lax.rsqrt(square - mean * mean + NORM_EPS)
+    with jax.named_scope("drain"):
+        settle(mixed_all.at[pl.ds(0, tps - 1)], send_sem.at[MIXED])
+        settle(route_all.at[pl.ds(0, eps - 1)], send_sem.at[ROUTE])
+        settle(weight_all.at[pl.ds(0, eps - 1)], send_sem.at[WEIGHT])
+        settle(side_out.at[pl.ds(0, eps - 1)], send_sem.at[SIDE])
+        settle(late_all.at[pl.ds(0, tps - 1)], send_sem.at[LATE])
+        settle(stats.at[pl.ds(0, tps - 1)], send_sem.at[STAT])
+        settle(hidden_all.at[:, pl.ds(0, tps - 1)], send_sem.at[HIDDEN])
+        settle(rows_all.at[pl.ds(0, 5), pl.ds(0, 6)], send_sem.at[7])
+        settle(rows_all.at[pl.ds(0, 4)], send_sem.at[8])
+        settle(pair_out, send_sem.at[9])
+        settle(line_out.at[pl.ds(0, steps - 1)], send_sem.at[10])
+
+
+def mixer(mixed, tokens, routes, route_weights, first_gain, side_switch, weights):
+    out_w, gate_w, up_w, down_w, shared_gate, _, shared_down, side_gate, _, side_down = weights
+    eps, tps = lax.axis_size("ep"), lax.axis_size("tp")
+    chips = eps // 2
+    rows, model = tokens.shape
+    cols = model // tps
+    experts, _, hidden = gate_w.shape
+    top = routes.shape[0]
+    total = experts * eps
+    capacity = (3 * rows * top + total - 1) // total
+    slots = -(-experts * capacity // 16) * 16
+    wide = -(-experts * rows // 128) * 128
+    side_width, side_rows = side_gate.shape
+    shared = shared_gate.shape[1]
+    bf16, f32 = jnp.bfloat16, jnp.float32
+    dma = pltpu.SemaphoreType.DMA
+    line = pltpu.VMEM((chips, rows, cols), bf16)
+    sides = pltpu.VMEM((eps, rows, 2 * side_width), bf16)
+    return pl.pallas_call(
+        functools.partial(mixer_body, (chips, tps, capacity)),
+        out_shape=jax.ShapeDtypeStruct((rows, cols), f32),
+        in_specs=[ANY] * 16,
+        out_specs=VMEM,
+        scratch_shapes=[
+            pltpu.VMEM((rows, cols), bf16),
+            pltpu.VMEM(first_gain.shape, f32),
+            pltpu.VMEM(side_switch.shape, bf16),
+            pltpu.VMEM((tps,) + mixed.shape, bf16),
+            pltpu.VMEM((eps, top, rows), jnp.int32),
+            pltpu.VMEM((eps, top, rows), f32),
+            pltpu.VMEM((eps, 2 * tps, rows, cols // 2), bf16),
+            pltpu.VMEM((eps * rows, model), bf16),
+            pltpu.VMEM((128, wide), f32),
+            pltpu.VMEM((wide, 128), f32),
+            pltpu.VMEM((2, tps, 4, slots, hidden), bf16),
+            line,
+            line,
+            line,
+            line,
+            pltpu.VMEM((chips, rows, cols), f32),
+            sides,
+            sides,
+            pltpu.VMEM((tps, rows, shared + 2 * side_width), bf16),
+            pltpu.VMEM((tps, 8, 128), f32),
+            pltpu.VMEM(out_w.shape, bf16),
+            pltpu.VMEM((experts, model, 2 * hidden), bf16),
+            pltpu.VMEM(down_w.shape, bf16),
+            pltpu.VMEM((model, 2 * shared), bf16),
+            pltpu.VMEM(shared_down.shape, bf16),
+            pltpu.VMEM((2 * side_width, side_rows), bf16),
+            pltpu.VMEM(side_down.shape, bf16),
+            dma((6,)),
+            dma((7,)),
+            dma((11,)),
+            dma((8,)),
+            dma((chips, 6)),
+            dma((5,)),
+        ],
+        compiler_params=pltpu.CompilerParams(collective_id=0, has_side_effects=True),
+    )(mixed, tokens, routes, route_weights, first_gain, side_switch, *weights)
+
+
+def streamed_device(
+    tokens,
+    retention_state,
+    lengths,
+    query_weight,
+    key_weight,
+    value_weight,
+    gate_weight,
+    out_weight,
+    first_gain,
+    routing,
+    route_weight,
+    expert_gate,
+    expert_up,
+    expert_down,
+    shared_gate,
+    shared_up,
+    shared_down,
+    side_gate,
+    side_up,
+    side_down,
+    side_switch,
+    second_gain,
+):
+    rows, heads, width = retention_state.shape[:3]
+    exponent = np.arange(width // 2, dtype=np.float64) / (width // 2)
+    frequency = np.tile((ROPE_BASE**-exponent).astype(np.float32), 2 * heads)[None, :]
+    mixed, new_state = retain_kernel(
+        tokens,
+        lengths.reshape(1, rows),
+        jnp.asarray(frequency),
+        [query_weight, key_weight, value_weight, gate_weight],
+        retention_state,
+    )
+    normed = mixer(
+        mixed,
+        tokens,
+        routing.T,
+        route_weight.T,
+        first_gain.reshape(1, -1),
+        side_switch,
+        [
+            out_weight,
+            expert_gate,
+            expert_up,
+            expert_down,
+            shared_gate,
+            shared_up,
+            shared_down,
+            side_gate.T,
+            side_up.T,
+            side_down,
+        ],
+    )
+    output = (normed * second_gain[None, :]).astype(jnp.bfloat16)
+    return (output, new_state)
+
+
+def staged_device(
     tokens,
     retention_state,
     lengths,
@@ -489,6 +1288,23 @@
     return (output, new_state)
 
 
+def on_device(*arrays):
+    tokens, state, expert_gate, side_gate = arrays[0], arrays[1], arrays[11], arrays[17]
+    eps, tps = lax.axis_size("ep"), lax.axis_size("tp")
+    rows, model = tokens.shape
+    fits = (
+        eps == 8
+        and tps == 4
+        and rows % 16 == 0
+        and model % (256 * tps) == 0
+        and state.shape[1] * state.shape[2] % 128 == 0
+        and expert_gate.shape[2] % 128 == 0
+        and side_gate.shape[0] % 128 == 0
+        and side_gate.shape[1] == 64
+    )
+    return (streamed_device if fits else staged_device)(*arrays)
+
+
 def solution(mesh):
     return jax.shard_map(
         on_device,

time: 125 us -> 57.8 us (0.46); the launches traced: 124 us -> 57.6 us
  other arithmetic: 22.4 us -> 1.52 us
  Pallas kernels: 76.2 us -> 55.4 us
  local copies, waits for them, and re-layouts: 12.2 us -> 0.01 us
  matrix products: 11.8 us -> 0 us
    pallas_call x7 -> x2, Pallas kernels: 76.2 us -> 55.4 us  [the longest x1 45.5 us: mixer(): pl.pallas_call(functools.partial(mixer_body, (chips, tps, capacity)), out...]
    dot_general x11 -> x0, matrix products: 11.8 us -> none  [the longest x1 1.75 us: on_device(): jnp.dot(normed_full, shared_up, preferred_element_type=jnp.float32)]
    add x2 -> x0, other arithmetic: 9.17 us -> none  [the longest x1 9.16 us: retain(): decays[None, :, None, None] * retention_state]
    reduce_sum x8 -> x0, other arithmetic: 4.89 us -> none  [the longest x2 1.4 us: row_moments(): totals = jnp.sum(every, 0)]
    convert_element_type x6 -> x1, other arithmetic: 5.02 us -> 1.52 us  [streamed_device(): output = (normed * second_gain[None, :]).astype(jnp.bfloat16)]
    unnamed x40 -> x2, local copies, waits for them, and re-layouts: 2.83 us -> 0.01 us
    reshape x3 -> x0, local copies, waits for them, and re-layouts: 2.53 us -> none  [the longest x1 0.84 us: retain(): key_part.reshape(row_count, head_count, head_width)]
    mul x6 -> x0, local copies, waits for them, and re-layouts: 1.78 us -> none  [the longest x2 0.85 us: retain(): own_term = jnp.sum(queries * key_rows, -1, keepdims=True) * values]
where the time goes in v2:
time: 57.8 us; the launch traced here: 57.6 us
  Pallas kernels  55.4 us (96%)
  other arithmetic  1.52 us (3%)
  between operations  0.66 us (1%)
    pallas_call x1, Pallas kernels, mixer(): pl.pallas_call(functools.partial(mixer_body, (chips, tps, capacity)), out...  45.5 us
    pallas_call x1, Pallas kernels, retain_kernel(): pl.pallas_call(functools.partial(retain_body, chunk), out_shape=[jax.Shap...  9.95 us
    convert_element_type x1, other arithmetic, streamed_device(): output = (normed * second_gain[None, :]).astype(jnp.bfloat16)  1.52 us

profile of v2, /device:TPU:0, one launch (start us, length us, event | category | flops | bytes accessed | tf_op | source)
XLA Modules:
  0.0 57.6 jit_solution(15044291807232570919)
XLA Ops:
  0.6 10.0 %shard_map.230 = (bf16[48,256]{1,0:T(8,128)(2,1)}, f32[48,4,64,64]{3,2,1,0:T(8,128)}) custom-call(bf16[48,2048]{1,0:T(8,128)(2,1)} %tokens_in.3, s32[1,48]{1,0:T(1,128)} %bitcast.11, f32[1,256]{1,0:T(1,128)} %constant.2.clone.frequency_in, bf16[2048,256]{1,0:T(8,128)(2,1)} %query_in.1, bf16[2048,256]{1,0:T(8,128)(2,1)} %key_in.1, ...), custom_call_target="tpu_custom_call" | custom-call | tf_op jit(solution)/shard_map/pallas_call | solution.py:515
  10.6 0.0 copy-start
  10.6 45.5 %shard_map.231 = f32[48,512]{1,0:T(8,128)} custom-call(bf16[48,256]{1,0:T(8,128)(2,1)} %get-tuple-element.4.mixed_in, bf16[48,2048]{1,0:T(8,128)(2,1)} %tokens_in.3, s32[4,48]{1,0:T(4,128)} %bitcast.9, f32[4,48]{1,0:T(4,128)} %bitcast.10, f32[1,2048]{1,0:T(1,128)} %bitcast.8, bf16[2048]{0:T(1024)(128)(2,1)} %side_switch_in.1, bf16[1024,512]{1,0:T(8,128)(2,1)} %out_in.1, ...), custom_call_target="tpu_custom_call" | custom-call | tf_op jit(solution)/shard_map/pallas_call | solution.py:1043
  56.1 0.0 copy-done
  56.1 1.5 %multiply_convert_fusion = bf16[48,512]{1,0:T(8,128)(2,1)} fusion(f32[48,512]{1,0:T(8,128)} %shard_map.231, f32[512]{0:T(512)S(1)} %copy-done), kind=kLoop, calls=%fused_computation | loop fusion | flops 49152 | bytes 149504 | tf_op jit(solution)/shard_map/convert_element_type | solution.py:1141
Async XLA Ops:
  10.6 45.5 %copy-start = (f32[512]{0:T(512)S(1)}, f32[512]{0:T(512)}, u32[]{:S(2)}) copy-start(f32[512]{0:T(512)} %param.44) | copy-start | bytes 6148

commit v3 on v2

--- a/solution.py
+++ b/solution.py
@@ -2,7 +2,6 @@
 
 import jax
 import jax.numpy as jnp
-import numpy as np
 from jax import lax
 from jax.experimental import pallas as pl
 from jax.experimental.pallas import tpu as pltpu
@@ -391,7 +390,6 @@
     chunk,
     tokens_in,
     lengths_in,
-    frequency_in,
     query_in,
     key_in,
     value_in,
@@ -401,7 +399,6 @@
     state_out,
     tokens,
     lengths,
-    frequency,
     weights,
     state,
     columns,
@@ -420,20 +417,23 @@
     small = [
         fetch(source, target, small_sem.at[i])
         for i, (source, target) in enumerate(
-            [(lengths_in, lengths), (frequency_in, frequency), (tokens_in, tokens)]
+            [(lengths_in, lengths), (tokens_in, tokens)]
         )
     ]
     for i, source in enumerate([query_in, key_in, value_in, gate_in]):
         fetch(source, weights.at[:, pl.ds(i * total, total)], weight_sem.at[i // 2])
+
+    with jax.named_scope("small_wait"):
+        small[0].wait()
     for i in range(chunks):
         piece = pl.ds(i * chunk, chunk)
         fetch(state_in.at[piece], state.at[piece], state_sem.at[i])
-
-    with jax.named_scope("small_wait"):
-        small[0].wait()
-        small[1].wait()
     position = column_of(lengths[...].astype(jnp.float32))
-    angles = position * frequency[...]
+    lane = lax.broadcasted_iota(jnp.int32, (1, total), 1) & (width // 2 - 1)
+    frequency = jnp.zeros((1, total), jnp.float32)
+    for i in range(width // 2):
+        frequency = jnp.where(lane == i, ROPE_BASE ** (-i / (width // 2)), frequency)
+    angles = position * frequency
     cosine, sine = jnp.cos(angles), jnp.sin(angles)
     first_head = lax.axis_index("tp") * heads
     decays = []
@@ -449,42 +449,37 @@
         return both[:, :total], both[:, total:]
 
     with jax.named_scope("small_wait"):
-        small[2].wait()
+        small[1].wait()
     query, key = project(0)
-    lanes = columns.shape[1] // 2
+    lanes = columns.shape[1]
     for i, (x, scale) in enumerate([(query, 1.0), (key, width ** (-0.5))]):
         turned = rotated(x, cosine, sine, width // 2) * scale
         padded = jnp.concatenate([turned, jnp.zeros((lanes - rows, total), jnp.float32)], 0)
-        flipped = jnp.transpose(padded)
-        high = flipped.astype(jnp.bfloat16)
-        columns[i * total : (i + 1) * total, :lanes] = high
-        columns[i * total : (i + 1) * total, lanes:] = (
-            flipped - high.astype(jnp.float32)
-        ).astype(jnp.bfloat16)
+        columns[i * total : (i + 1) * total, :] = jnp.transpose(padded).astype(jnp.bfloat16)
     value, gate = project(1)
     for head in range(heads):
         values[head] = value[:, head * width : (head + 1) * width]
 
-    source_lane = lax.broadcasted_iota(jnp.int32, (2 * lanes, 2 * lanes), 0) & (lanes - 1)
-    target_lane = lax.broadcasted_iota(jnp.int32, (2 * lanes, 2 * lanes), 1)
+    source_lane = lax.broadcasted_iota(jnp.int32, (lanes, 2 * lanes), 0)
+    target_lane = lax.broadcasted_iota(jnp.int32, (lanes, 2 * lanes), 1)
     offset = jnp.where(target_lane >= lanes, 1, 0)
     buffers = [spread_even, spread_odd]
 
-    def widen(i):
-        for pair in range(chunk // 2):
-            pick = jnp.where(source_lane == offset + (i * chunk + 2 * pair), 1.0, 0.0)
-            buffers[i % 2][pair] = dot(columns[...], pick.astype(jnp.bfloat16))
-
-    widen(0)
+    def widen(i, pair):
+        pick = jnp.where(source_lane == offset + (i * chunk + 2 * pair), 1.0, 0.0)
+        buffers[i % 2][pair] = dot(columns[...], pick.astype(jnp.bfloat16))
+
+    for pair in range(chunk // 2):
+        widen(0, pair)
     for i in range(chunks):
         base = i * chunk
         piece = pl.ds(base, chunk)
         with jax.named_scope("state_wait"):
             pltpu.make_async_copy(state_in.at[piece], state.at[piece], state_sem.at[i]).wait()
-        if i + 1 < chunks:
-            widen(i + 1)
         wide = buffers[i % 2]
         for at in range(chunk):
+            if i + 1 < chunks and at % 2 == 0:
+                widen(i + 1, at // 2)
             lane = (at % 2) * lanes
             for head in range(heads):
                 low, high = head * width, (head + 1) * width
@@ -507,7 +502,7 @@
         settle(state, out_sem)
 
 
-def retain_kernel(tokens, lengths, frequency, weights, state):
+def retain_kernel(tokens, lengths, weights, state):
     rows, heads, width = state.shape[0], state.shape[1], state.shape[2]
     chunk, lanes = 8, 128
     cols = heads * width
@@ -518,25 +513,25 @@
             jax.ShapeDtypeStruct((rows, cols), jnp.bfloat16),
             jax.ShapeDtypeStruct(state.shape, state.dtype),
         ],
-        in_specs=[ANY] * 8,
+        in_specs=[ANY] * 7,
         out_specs=[VMEM, ANY],
+        compiler_params=pltpu.CompilerParams(vmem_limit_bytes=55200 * 2**10),
         scratch_shapes=[
             pltpu.VMEM(tokens.shape, tokens.dtype),
             pltpu.VMEM(lengths.shape, lengths.dtype),
-            pltpu.VMEM(frequency.shape, frequency.dtype),
             pltpu.VMEM((tokens.shape[1], 4 * cols), jnp.bfloat16),
             pltpu.VMEM(state.shape, state.dtype),
-            pltpu.VMEM((2 * cols, 2 * lanes), jnp.bfloat16),
+            pltpu.VMEM((2 * cols, lanes), jnp.bfloat16),
             wide,
             wide,
             pltpu.VMEM((heads, rows, width), jnp.float32),
             pltpu.VMEM((heads, rows, width), jnp.float32),
-            pltpu.SemaphoreType.DMA((3,)),
+            pltpu.SemaphoreType.DMA((2,)),
             pltpu.SemaphoreType.DMA((2,)),
             pltpu.SemaphoreType.DMA((rows // chunk,)),
             pltpu.SemaphoreType.DMA,
         ],
-    )(tokens, lengths, frequency, *weights, state)
+    )(tokens, lengths, *weights, state)
 
 
 def mixer_body(
@@ -592,13 +587,14 @@
     row_sem,
     back_sem,
 ):
-    chips, tps, capacity = dims
+    chips, tps, capacity, groups = dims
     steps = chips
     rows, cols = own_tokens.shape
     model = cols * tps
     half = cols // 2
     experts, hidden_width = gate_in.shape[0], gate_in.shape[2]
-    slots = hidden_all.shape[3]
+    slots = experts * capacity
+    pair_slots = hidden_all.shape[2]
     side_width = side_gate_in.shape[0]
     side_rows = side_gate_in.shape[1]
     shared_width = shared_gate_in.shape[1]
@@ -634,11 +630,18 @@
 
     own_mixed = mixed_all.at[tp]
     own_slice = pl.ds(pl.multiple_of(tp * cols, cols), cols)
-    fetch(mixed_in, own_mixed, small_sem.at[0])
     fetch(routes_in, route_all.at[ep], small_sem.at[1])
     fetch(route_weights_in, weight_all.at[ep], small_sem.at[2])
     fetch(tokens_in.at[:, own_slice], own_tokens, small_sem.at[3])
     fetch(out_in, out_w, weight_sem.at[0])
+    MIXED, ROUTE, WEIGHT, SIDE, LATE, STAT, HIDDEN = 0, 1, 2, 3, 4, 5, 6
+
+    def push(source, target, sent, received, peer):
+        send(source, target, sent, received, peer)
+
+    with jax.named_scope("small_wait"):
+        settle(route_all.at[ep], small_sem.at[1])
+        settle(weight_all.at[ep], small_sem.at[2])
     fetch(first_gain_in, first_gain, small_sem.at[4])
     fetch(side_switch_in, side_switch, small_sem.at[5])
     for e in range(experts):
@@ -651,27 +654,18 @@
     fetch(down_in, down_w, weight_sem.at[4])
     fetch(shared_down_in, shared_down_w, weight_sem.at[5])
     fetch(side_down_in, side_down_w, weight_sem.at[6])
-
-    MIXED, ROUTE, WEIGHT, SIDE, LATE, STAT, HIDDEN = 0, 1, 2, 3, 4, 5, 6
-
-    def push(source, target, sent, received, peer):
-        send(source, target, sent, received, peer)
-
-    with jax.named_scope("small_wait"):
-        settle(own_mixed, small_sem.at[0])
-        settle(route_all.at[ep], small_sem.at[1])
-        settle(weight_all.at[ep], small_sem.at[2])
     with jax.named_scope("enter"):
         pl.semaphore_wait(barrier, len(peers))
 
     for peer in plane:
-        push(own_mixed, own_mixed, send_sem.at[MIXED], recv_sem.at[MIXED], peer)
+        push(mixed_in, own_mixed, send_sem.at[MIXED], recv_sem.at[MIXED], peer)
     for peer in others:
         own = route_all.at[ep]
         push(own, own, send_sem.at[ROUTE], recv_sem.at[ROUTE], peer)
         own = weight_all.at[ep]
         push(own, own, send_sem.at[WEIGHT], recv_sem.at[WEIGHT], peer)
 
+    mixed_all[tp] = mixed_in[...]
     with jax.named_scope("out_wait"):
         settle(own_tokens, small_sem.at[3])
         settle(out_w, weight_sem.at[0])
@@ -701,22 +695,18 @@
         ref = block(step, tp)
         if step > 0:
             came(ref, step, 0)
-        push_rows(ref, step, 1, plane[0])
-        push_rows(ref, step, 2, plane[1])
+        for i, peer in enumerate(plane):
+            push_rows(ref, step, 1 + i, peer)
         push_rows(ref, step, 5, partner)
 
     def relay(step):
-        came(block(step, tp_x), step, 1)
-        push_rows(piece(step, tp_x, 0), step, 3, plane[1])
-        push_rows(block(step, tp_x), step, 5, partner)
-        came(block(step, tp_y), step, 2)
-        push_rows(piece(step, tp_y, 1), step, 4, plane[0])
-        push_rows(block(step, tp_y), step, 5, partner)
+        for i, index in enumerate([tp_x, tp_y]):
+            came(block(step, index), step, 1 + i)
+            push_rows(block(step, index), step, 5, partner)
 
     def corner(step):
-        for part in range(2):
-            came(piece(step, tp_d, part), step, 3 + part)
-            push_rows(piece(step, tp_d, part), step, 5, partner)
+        came(block(step, tp_d), step, 3)
+        push_rows(block(step, tp_d), step, 5, partner)
 
     def arrive(step):
         came(rows_all.at[group_at(step, 1)], step, 5)
@@ -766,7 +756,13 @@
     side_span = pl.ds(pl.multiple_of(ep * side_rows, side_rows), side_rows)
 
     def blocks(group):
-        return [(step, at) for step in (2 * group, 2 * group + 1) for at in range(2)]
+        return [(step, at) for step in groups[group] for at in range(2)]
+
+    def group_rows(group):
+        return slice(2 * groups[group][0] * rows, 2 * (groups[group][-1] + 1) * rows)
+
+    def group_steps(group):
+        return pl.ds(groups[group][0], len(groups[group]))
 
     def norm_step(step, at):
         g, base = group_at(step, at), (2 * step + at) * rows
@@ -788,9 +784,8 @@
     def side_step(group):
         if group == 0:
             settle(side_w, weight_sem.at[2])
-        first = 4 * group * rows
         partial = lax.dot_general(
-            normed[first : first + 4 * rows, side_span],
+            normed[group_rows(group), side_span],
             side_w[...],
             (((1,), (1,)), ((), ())),
             preferred_element_type=jnp.float32,
@@ -811,36 +806,44 @@
     def expert_step(group):
         if group == 0:
             settle(gate_up_w, weight_sem.at[1])
-        first = 4 * group * rows
-        stacks = [[] for _ in range(4)]
-        scales = [column(eps + group_at(step, at)) for step, at in blocks(group)]
+        members = blocks(group)
+        stacks = [[] for _ in members]
+        scales = [column(eps + group_at(step, at)) for step, at in members]
         for e in range(experts):
-            both = dot(normed[first : first + 4 * rows, :], gate_up_w[e])
+            both = dot(normed[group_rows(group), :], gate_up_w[e])
             hidden = silu(both[:, :hidden_width]) * both[:, hidden_width:]
-            for i in range(4):
+            for i in range(len(members)):
                 mine = hidden[i * rows : (i + 1) * rows] * scales[i][e * rows : (e + 1) * rows]
                 stacks[i].append(mine.astype(jnp.bfloat16))
-        for i, (step, at) in enumerate(blocks(group)):
-            slot_row = info[pl.ds(group_at(step, at), 1), 0:wide]
-            number = lax.broadcasted_iota(jnp.int32, (slots, wide), 0).astype(jnp.float32)
+        number = lax.broadcasted_iota(jnp.int32, (pair_slots, 2 * wide), 0).astype(jnp.float32)
+        for i, step in enumerate(groups[group]):
+            near = info[pl.ds(group_at(step, 0), 1), 0:wide]
+            far = info[pl.ds(group_at(step, 1), 1), 0:wide]
+            far = jnp.where(far < 0.0, -1.0, far + slots)
+            slot_row = jnp.concatenate([near, far], 1)
             table = jnp.where(number == slot_row, 1.0, 0.0).astype(jnp.bfloat16)
-            packed = dot(table, jnp.concatenate(stacks[i], 0)).astype(jnp.bfloat16)
-            hidden_all[group, tp, i] = packed
-        own = hidden_all.at[group, tp]
+            stack = jnp.concatenate(stacks[2 * i] + stacks[2 * i + 1], 0)
+            hidden_all[tp, step] = dot(table, stack).astype(jnp.bfloat16)
+        own = hidden_all.at[tp, group_steps(group)]
         for peer in plane:
             push(own, own, send_sem.at[HIDDEN], recv_sem.at[HIDDEN + group], peer)
 
     def down_step(group):
         with jax.named_scope("hidden_wait"):
-            settle(hidden_all.at[group, pl.ds(0, tps - 1)], recv_sem.at[HIDDEN + group])
+            arrived = hidden_all.at[pl.ds(0, tps - 1), group_steps(group)]
+            settle(arrived, recv_sem.at[HIDDEN + group])
         if group == 0:
             settle(down_w, weight_sem.at[4])
         spread_rows = []
-        for i, (step, at) in enumerate(blocks(group)):
-            number = lax.broadcasted_iota(jnp.int32, (wide, slots), 1).astype(jnp.float32)
-            table = jnp.where(number == column(group_at(step, at)), 1.0, 0.0).astype(jnp.bfloat16)
-            packed = jnp.concatenate([hidden_all[group, t, i] for t in range(tps)], 1)
-            spread_rows.append(dot(table, packed).astype(jnp.bfloat16))
+        number = lax.broadcasted_iota(jnp.int32, (wide, pair_slots), 1).astype(jnp.float32)
+        for step in groups[group]:
+            packed = jnp.concatenate([hidden_all[t, step] for t in range(tps)], 1)
+            for at in range(2):
+                slot = column(group_at(step, at))
+                if at == 1:
+                    slot = jnp.where(slot < 0.0, -1.0, slot + slots)
+                table = jnp.where(number == slot, 1.0, 0.0).astype(jnp.bfloat16)
+                spread_rows.append(dot(table, packed).astype(jnp.bfloat16))
         result = None
         for e in range(experts):
             mine = jnp.concatenate([r[e * rows : (e + 1) * rows] for r in spread_rows], 0)
@@ -852,7 +855,7 @@
                 total[step] = part
             else:
                 pair_out[step] = part.astype(jnp.bfloat16)
-        both = pl.ds(2 * group, 2)
+        both = group_steps(group)
         push(
             pair_out.at[both],
             pair_in.at[both],
@@ -862,10 +865,10 @@
         )
 
     def return_step(group):
-        both = pl.ds(2 * group, 2)
+        both = group_steps(group)
         with jax.named_scope("pair_wait"):
             settle(pair_in.at[both], back_sem.at[group])
-        for step in (2 * group, 2 * group + 1):
+        for step in groups[group]:
             mine = total[step] + pair_in[step].astype(jnp.float32)
             if step == 0:
                 total[step] = mine
@@ -875,7 +878,7 @@
                 line_out.at[step],
                 line_in.at[step],
                 send_sem.at[10],
-                back_sem.at[1 + step],
+                back_sem.at[steps + step],
                 line[step],
             )
 
@@ -962,37 +965,45 @@
         norm_step(2, 0)
     with jax.named_scope("norm_step2_1"):
         norm_step(2, 1)
-    with jax.named_scope("own_shared"):
-        own_shared()
+    with jax.named_scope("side_step1"):
+        side_step(1)
+    with jax.named_scope("expert_step1"):
+        expert_step(1)
     with jax.named_scope("arrive3"):
         arrive(3)
     with jax.named_scope("norm_step3_0"):
         norm_step(3, 0)
     with jax.named_scope("norm_step3_1"):
         norm_step(3, 1)
-    with jax.named_scope("side_step1"):
-        side_step(1)
-    with jax.named_scope("expert_step1"):
-        expert_step(1)
+    with jax.named_scope("side_step2"):
+        side_step(2)
+    with jax.named_scope("expert_step2"):
+        expert_step(2)
     with jax.named_scope("down_step0"):
         down_step(0)
+    with jax.named_scope("own_shared"):
+        own_shared()
+    with jax.named_scope("own_switch"):
+        switch = own_switch()
     with jax.named_scope("return_step0"):
         return_step(0)
-    with jax.named_scope("own_switch"):
-        switch = own_switch()
+    with jax.named_scope("down_step1"):
+        down_step(1)
     with jax.named_scope("own_side"):
         own_side()
-    with jax.named_scope("down_step1"):
-        down_step(1)
+    with jax.named_scope("return_step1"):
+        return_step(1)
+    with jax.named_scope("down_step2"):
+        down_step(2)
+    with jax.named_scope("return_step2"):
+        return_step(2)
     with jax.named_scope("own_extra"):
         extra = own_extra()
-    with jax.named_scope("return_step1"):
-        return_step(1)
 
     routed = total[0]
     for step in range(1, steps):
         with jax.named_scope("line_wait"):
-            settle(line_in.at[step], back_sem.at[1 + step])
+            settle(line_in.at[step], back_sem.at[steps + step])
         routed = routed + line_in[step].astype(jnp.float32)
     own = normed[0:rows, own_slice].astype(jnp.float32)
     pre_second = RESIDUAL_SCALE * own + routed + extra
@@ -1015,7 +1026,7 @@
         settle(side_out.at[pl.ds(0, eps - 1)], send_sem.at[SIDE])
         settle(late_all.at[pl.ds(0, tps - 1)], send_sem.at[LATE])
         settle(stats.at[pl.ds(0, tps - 1)], send_sem.at[STAT])
-        settle(hidden_all.at[:, pl.ds(0, tps - 1)], send_sem.at[HIDDEN])
+        settle(hidden_all.at[pl.ds(0, tps - 1)], send_sem.at[HIDDEN])
         settle(rows_all.at[pl.ds(0, 5), pl.ds(0, 6)], send_sem.at[7])
         settle(rows_all.at[pl.ds(0, 4)], send_sem.at[8])
         settle(pair_out, send_sem.at[9])
@@ -1032,7 +1043,8 @@
     top = routes.shape[0]
     total = experts * eps
     capacity = (3 * rows * top + total - 1) // total
-    slots = -(-experts * capacity // 16) * 16
+    slots = -(-2 * experts * capacity // 16) * 16
+    groups = ((0, 1), (2,), (3,))
     wide = -(-experts * rows // 128) * 128
     side_width, side_rows = side_gate.shape
     shared = shared_gate.shape[1]
@@ -1041,9 +1053,9 @@
     line = pltpu.VMEM((chips, rows, cols), bf16)
     sides = pltpu.VMEM((eps, rows, 2 * side_width), bf16)
     return pl.pallas_call(
-        functools.partial(mixer_body, (chips, tps, capacity)),
+        functools.partial(mixer_body, (chips, tps, capacity, groups)),
         out_shape=jax.ShapeDtypeStruct((rows, cols), f32),
-        in_specs=[ANY] * 16,
+        in_specs=[VMEM] + [ANY] * 15,
         out_specs=VMEM,
         scratch_shapes=[
             pltpu.VMEM((rows, cols), bf16),
@@ -1056,7 +1068,7 @@
             pltpu.VMEM((eps * rows, model), bf16),
             pltpu.VMEM((128, wide), f32),
             pltpu.VMEM((wide, 128), f32),
-            pltpu.VMEM((2, tps, 4, slots, hidden), bf16),
+            pltpu.VMEM((tps, chips, slots, hidden), bf16),
             line,
             line,
             line,
@@ -1076,11 +1088,13 @@
             dma((6,)),
             dma((7,)),
             dma((11,)),
-            dma((8,)),
+            dma((6 + len(groups),)),
             dma((chips, 6)),
-            dma((5,)),
+            dma((2 * chips,)),
         ],
-        compiler_params=pltpu.CompilerParams(collective_id=0, has_side_effects=True),
+        compiler_params=pltpu.CompilerParams(
+            collective_id=0, has_side_effects=True, vmem_limit_bytes=54900 * 2**10
+        ),
     )(mixed, tokens, routes, route_weights, first_gain, side_switch, *weights)
 
 
@@ -1108,13 +1122,10 @@
     side_switch,
     second_gain,
 ):
-    rows, heads, width = retention_state.shape[:3]
-    exponent = np.arange(width // 2, dtype=np.float64) / (width // 2)
-    frequency = np.tile((ROPE_BASE**-exponent).astype(np.float32), 2 * heads)[None, :]
+    rows = tokens.shape[0]
     mixed, new_state = retain_kernel(
         tokens,
         lengths.reshape(1, rows),
-        jnp.asarray(frequency),
         [query_weight, key_weight, value_weight, gate_weight],
         retention_state,
     )

time: 57.8 us -> 50.6 us (0.88)
  Pallas kernels: 55.4 us -> 48.4 us
  other arithmetic: 1.52 us -> 0.63 us
  local copies, waits for them, and re-layouts: 0.01 us -> 0.68 us
    pallas_call x1, Pallas kernels: 45.5 us -> 40.7 us  [mixer(): pl.pallas_call(functools.partial(mixer_body, (chips, tps, capacity, group...]
    pallas_call x1, Pallas kernels: 9.95 us -> 7.7 us  [retain_kernel(): pl.pallas_call(functools.partial(retain_body, chunk), out_shape=[jax.Shap...]
    convert_element_type x1, other arithmetic: 1.52 us -> 0.63 us  [streamed_device(): output = (normed * second_gain[None, :]).astype(jnp.bfloat16)]
    unnamed x2 -> x16, local copies, waits for them, and re-layouts: 0.01 us -> 0.68 us
where the time goes in v3:
time: 50.6 us; the launch traced here: 50.4 us
  Pallas kernels  48.4 us (96%)
  between operations  0.74 us (1%)
  local copies, waits for them, and re-layouts  0.68 us (1%)
  other arithmetic  0.63 us (1%)
    pallas_call x1, Pallas kernels, mixer(): pl.pallas_call(functools.partial(mixer_body, (chips, tps, capacity, group...  40.7 us
    pallas_call x1, Pallas kernels, retain_kernel(): pl.pallas_call(functools.partial(retain_body, chunk), out_shape=[jax.Shap...  7.7 us

profile of v3, /device:TPU:0, one launch (start us, length us, event | category | flops | bytes accessed | tf_op | source)
XLA Modules:
  0.0 50.4 jit_solution(5275635713976654959)
XLA Ops:
  0.6 0.0 copy-start.6
  0.6 0.6 %copy-done.6 = s32[48]{0:T(128)S(1)} copy-done((s32[48]{0:T(128)S(1)}, s32[48]{0:T(128)}, u32[]{:S(2)}) %copy-start.6) | copy-done | bytes 216
  1.3 0.0 copy-start
  1.3 0.0 copy-start.1
  1.3 0.0 copy-start.2
  1.3 0.0 copy-start.3
  1.3 0.0 copy-start.4
  1.3 0.0 copy-start.5
  1.3 7.7 %shard_map.221 = (bf16[48,256]{1,0:T(8,128)(2,1)S(1)}, f32[48,4,64,64]{3,2,1,0:T(8,128)}) custom-call(bf16[48,2048]{1,0:T(8,128)(2,1)} %tokens_in.3, s32[1,48]{1,0:T(1,128)S(1)} %bitcast.11, bf16[2048,256]{1,0:T(8,128)(2,1)} %query_in.1, bf16[2048,256]{1,0:T(8,128)(2,1)} %key_in.1, bf16[2048,256]{1,0:T(8,128)(2,1)} %value_in.1, bf16[2048,256]{1,0:T(8,128)(2,1)} %gate_in.2, ...), custom_call_target="tpu_custom_call" | custom-call | tf_op jit(solution)/shard_map/pallas_call | solution.py:510
  9.0 0.0 copy-done
  9.0 0.0 copy-done.1
  9.1 0.0 copy-done.2
  9.1 0.0 copy-done.3
  9.1 0.0 copy-done.4
  9.1 0.0 copy-done.5
  9.1 0.0 copy-start.7
  9.1 40.7 %shard_map.222 = f32[48,512]{1,0:T(8,128)S(1)} custom-call(bf16[48,256]{1,0:T(8,128)(2,1)S(1)} %get-tuple-element.4.mixed_in, bf16[48,2048]{1,0:T(8,128)(2,1)} %tokens_in.3, s32[4,48]{1,0:T(4,128)S(1)} %bitcast.9, f32[4,48]{1,0:T(4,128)S(1)} %bitcast.10, f32[1,2048]{1,0:T(1,128)S(1)} %bitcast.8, bf16[2048]{0:T(1024)(128)(2,1)S(1)} %copy-done.3, ...), custom_call_target="tpu_custom_call" | custom-call | tf_op jit(solution)/shard_map/pallas_call | solution.py:1055
  49.8 0.0 copy-done.7
  49.8 0.6 %multiply_convert_fusion = bf16[48,512]{1,0:T(8,128)(2,1)} fusion(f32[48,512]{1,0:T(8,128)S(1)} %shard_map.222, f32[512]{0:T(512)S(1)} %copy-done.7), kind=kLoop, calls=%fused_computation | loop fusion | flops 49152 | bytes 149504 | tf_op jit(solution)/shard_map/convert_element_type | solution.py:1152
Async XLA Ops:
  0.6 0.7 %copy-start.6 = (s32[48]{0:T(128)S(1)}, s32[48]{0:T(128)}, u32[]{:S(2)}) copy-start(s32[48]{0:T(128)} %param.24) | copy-start | bytes 580
  1.3 7.7 %copy-start = (bf16[256,64]{0,1:T(8,128)(2,1)S(1)}, bf16[256,64]{0,1:T(8,128)(2,1)}, u32[]{:S(2)}) copy-start(bf16[256,64]{0,1:T(8,128)(2,1)} %param.39) | copy-start | bytes 98308
  1.3 7.8 %copy-start.1 = (bf16[256,64]{0,1:T(8,128)(2,1)S(1)}, bf16[256,64]{0,1:T(8,128)(2,1)}, u32[]{:S(2)}) copy-start(bf16[256,64]{0,1:T(8,128)(2,1)} %param.40) | copy-start | bytes 98308
  1.3 7.8 %copy-start.2 = (f32[2048]{0:T(1024)S(1)}, f32[2048]{0:T(1024)}, u32[]{:S(2)}) copy-start(f32[2048]{0:T(1024)} %param.30) | copy-start | bytes 24580
  1.3 7.8 %copy-start.3 = (bf16[2048]{0:T(1024)(128)(2,1)S(1)}, bf16[2048]{0:T(1024)(128)(2,1)}, u32[]{:S(2)}) copy-start(bf16[2048]{0:T(1024)(128)(2,1)} %side_switch_in.1) | copy-start | bytes 12292
  1.3 7.8 %copy-start.4 = (s32[48,4]{0,1:T(4,128)S(1)}, s32[48,4]{0,1:T(4,128)}, u32[]{:S(2)}) copy-start(s32[48,4]{0,1:T(4,128)} %param.31) | copy-start | bytes 2308
  1.3 7.8 %copy-start.5 = (f32[48,4]{0,1:T(4,128)S(1)}, f32[48,4]{0,1:T(4,128)}, u32[]{:S(2)}) copy-start(f32[48,4]{0,1:T(4,128)} %param.32) | copy-start | bytes 2308
  9.1 40.7 %copy-start.7 = (f32[512]{0:T(512)S(1)}, f32[512]{0:T(512)}, u32[]{:S(2)}) copy-start(f32[512]{0:T(512)} %param.43) | copy-start | bytes 6148

commit v4 on v3

--- a/solution.py
+++ b/solution.py
@@ -451,12 +451,12 @@
     with jax.named_scope("small_wait"):
         small[1].wait()
     query, key = project(0)
+    value, gate = project(1)
     lanes = columns.shape[1]
     for i, (x, scale) in enumerate([(query, 1.0), (key, width ** (-0.5))]):
         turned = rotated(x, cosine, sine, width // 2) * scale
         padded = jnp.concatenate([turned, jnp.zeros((lanes - rows, total), jnp.float32)], 0)
         columns[i * total : (i + 1) * total, :] = jnp.transpose(padded).astype(jnp.bfloat16)
-    value, gate = project(1)
     for head in range(heads):
         values[head] = value[:, head * width : (head + 1) * width]
 
@@ -465,12 +465,13 @@
     offset = jnp.where(target_lane >= lanes, 1, 0)
     buffers = [spread_even, spread_odd]
 
-    def widen(i, pair):
+    def widen(i, pair, half):
         pick = jnp.where(source_lane == offset + (i * chunk + 2 * pair), 1.0, 0.0)
-        buffers[i % 2][pair] = dot(columns[...], pick.astype(jnp.bfloat16))
-
-    for pair in range(chunk // 2):
-        widen(0, pair)
+        span = slice(half * total, (half + 1) * total)
+        buffers[i % 2][pair, span] = dot(columns[span, :], pick.astype(jnp.bfloat16))
+
+    for pair in range(chunk):
+        widen(0, pair // 2, pair % 2)
     for i in range(chunks):
         base = i * chunk
         piece = pl.ds(base, chunk)
@@ -478,8 +479,11 @@
             pltpu.make_async_copy(state_in.at[piece], state.at[piece], state_sem.at[i]).wait()
         wide = buffers[i % 2]
         for at in range(chunk):
-            if i + 1 < chunks and at % 2 == 0:
-                widen(i + 1, at // 2)
+            if i + 1 < chunks:
+                widen(i + 1, at // 2, at % 2)
+            if at == chunk // 2:
+                part = pl.ds(base, chunk // 2)
+                fetch(state.at[part], state_out.at[part], out_sem)
             lane = (at % 2) * lanes
             for head in range(heads):
                 low, high = head * width, (head + 1) * width
@@ -491,7 +495,8 @@
                 carried[head, base + at : base + at + 1, :] = jnp.sum(
                     q_cols * new, 0, keepdims=True
                 )
-        fetch(state.at[piece], state_out.at[piece], out_sem)
+        part = pl.ds(base + chunk // 2, chunk // 2)
+        fetch(state.at[part], state_out.at[part], out_sem)
     parts = []
     for head in range(heads):
         result = carried[head]
@@ -925,78 +930,86 @@
         relay(0)
     with jax.named_scope("spread1"):
         spread(1)
+    with jax.named_scope("corner0"):
+        corner(0)
     with jax.named_scope("spread2"):
         spread(2)
-    with jax.named_scope("corner0"):
-        corner(0)
     with jax.named_scope("relay1"):
         relay(1)
-    with jax.named_scope("spread3"):
-        spread(3)
     with jax.named_scope("arrive0"):
         arrive(0)
     with jax.named_scope("norm_step0_0"):
         norm_step(0, 0)
     with jax.named_scope("norm_step0_1"):
         norm_step(0, 1)
+    with jax.named_scope("side_step0"):
+        side_step(0)
+    with jax.named_scope("expert_step0"):
+        expert_step(0)
+    with jax.named_scope("corner1"):
+        corner(1)
+    with jax.named_scope("spread3"):
+        spread(3)
     with jax.named_scope("relay2"):
         relay(2)
-    with jax.named_scope("corner1"):
-        corner(1)
-    with jax.named_scope("relay3"):
-        relay(3)
     with jax.named_scope("arrive1"):
         arrive(1)
     with jax.named_scope("norm_step1_0"):
         norm_step(1, 0)
     with jax.named_scope("norm_step1_1"):
         norm_step(1, 1)
-    with jax.named_scope("side_step0"):
-        side_step(0)
-    with jax.named_scope("expert_step0"):
-        expert_step(0)
+    with jax.named_scope("side_step1"):
+        side_step(1)
+    with jax.named_scope("expert_step1"):
+        expert_step(1)
     with jax.named_scope("corner2"):
         corner(2)
-    with jax.named_scope("corner3"):
-        corner(3)
+    with jax.named_scope("relay3"):
+        relay(3)
     with jax.named_scope("arrive2"):
         arrive(2)
     with jax.named_scope("norm_step2_0"):
         norm_step(2, 0)
     with jax.named_scope("norm_step2_1"):
         norm_step(2, 1)
-    with jax.named_scope("side_step1"):
-        side_step(1)
-    with jax.named_scope("expert_step1"):
-        expert_step(1)
+    with jax.named_scope("side_step2"):
+        side_step(2)
+    with jax.named_scope("expert_step2"):
+        expert_step(2)
+    with jax.named_scope("corner3"):
+        corner(3)
     with jax.named_scope("arrive3"):
         arrive(3)
     with jax.named_scope("norm_step3_0"):
         norm_step(3, 0)
     with jax.named_scope("norm_step3_1"):
         norm_step(3, 1)
-    with jax.named_scope("side_step2"):
-        side_step(2)
-    with jax.named_scope("expert_step2"):
-        expert_step(2)
+    with jax.named_scope("side_step3"):
+        side_step(3)
+    with jax.named_scope("expert_step3"):
+        expert_step(3)
     with jax.named_scope("down_step0"):
         down_step(0)
+    with jax.named_scope("down_step1"):
+        down_step(1)
     with jax.named_scope("own_shared"):
         own_shared()
     with jax.named_scope("own_switch"):
         switch = own_switch()
     with jax.named_scope("return_step0"):
         return_step(0)
-    with jax.named_scope("down_step1"):
-        down_step(1)
-    with jax.named_scope("own_side"):
-        own_side()
     with jax.named_scope("return_step1"):
         return_step(1)
     with jax.named_scope("down_step2"):
         down_step(2)
+    with jax.named_scope("own_side"):
+        own_side()
     with jax.named_scope("return_step2"):
         return_step(2)
+    with jax.named_scope("down_step3"):
+        down_step(3)
+    with jax.named_scope("return_step3"):
+        return_step(3)
     with jax.named_scope("own_extra"):
         extra = own_extra()
 
@@ -1044,7 +1057,7 @@
     total = experts * eps
     capacity = (3 * rows * top + total - 1) // total
     slots = -(-2 * experts * capacity // 16) * 16
-    groups = ((0, 1), (2,), (3,))
+    groups = ((0,), (1,), (2,), (3,))
     wide = -(-experts * rows // 128) * 128
     side_width, side_rows = side_gate.shape
     shared = shared_gate.shape[1]

time: 50.6 us -> 49.3 us (0.974)
  Pallas kernels: 48.4 us -> 47.1 us
    pallas_call x1, Pallas kernels: 40.7 us -> 39.8 us  [mixer(): pl.pallas_call(functools.partial(mixer_body, (chips, tps, capacity, group...]
where the time goes in v4:
time: 49.3 us; the launch traced here: 49.1 us
  Pallas kernels  47.1 us (96%)
  between operations  0.74 us (2%)
  local copies, waits for them, and re-layouts  0.68 us (1%)
  other arithmetic  0.63 us (1%)
    pallas_call x1, Pallas kernels, mixer(): pl.pallas_call(functools.partial(mixer_body, (chips, tps, capacity, group...  39.8 us
    pallas_call x1, Pallas kernels, retain_kernel(): pl.pallas_call(functools.partial(retain_body, chunk), out_shape=[jax.Shap...  7.27 us

profile of v4, /device:TPU:0, one launch (start us, length us, event | category | flops | bytes accessed | tf_op | source)
XLA Modules:
  0.0 49.1 jit_solution(4245313751406210034)
XLA Ops:
  0.6 0.0 copy-start.6
  0.6 0.6 %copy-done.6 = s32[48]{0:T(128)S(1)} copy-done((s32[48]{0:T(128)S(1)}, s32[48]{0:T(128)}, u32[]{:S(2)}) %copy-start.6) | copy-done | bytes 216
  1.3 0.0 copy-start
  1.3 0.0 copy-start.1
  1.3 0.0 copy-start.2
  1.3 0.0 copy-start.3
  1.3 0.0 copy-start.4
  1.3 0.0 copy-start.5
  1.3 7.3 %shard_map.221 = (bf16[48,256]{1,0:T(8,128)(2,1)S(1)}, f32[48,4,64,64]{3,2,1,0:T(8,128)}) custom-call(bf16[48,2048]{1,0:T(8,128)(2,1)} %tokens_in.3, s32[1,48]{1,0:T(1,128)S(1)} %bitcast.11, bf16[2048,256]{1,0:T(8,128)(2,1)} %query_in.1, bf16[2048,256]{1,0:T(8,128)(2,1)} %key_in.1, bf16[2048,256]{1,0:T(8,128)(2,1)} %value_in.1, bf16[2048,256]{1,0:T(8,128)(2,1)} %gate_in.2, ...), custom_call_target="tpu_custom_call" | custom-call | tf_op jit(solution)/shard_map/pallas_call | solution.py:515
  8.6 0.0 copy-done
  8.6 0.0 copy-done.1
  8.6 0.0 copy-done.2
  8.6 0.0 copy-done.3
  8.6 0.0 copy-done.4
  8.7 0.0 copy-done.5
  8.7 0.0 copy-start.7
  8.7 39.8 %shard_map.222 = f32[48,512]{1,0:T(8,128)S(1)} custom-call(bf16[48,256]{1,0:T(8,128)(2,1)S(1)} %get-tuple-element.4.mixed_in, bf16[48,2048]{1,0:T(8,128)(2,1)} %tokens_in.3, s32[4,48]{1,0:T(4,128)S(1)} %bitcast.9, f32[4,48]{1,0:T(4,128)S(1)} %bitcast.10, f32[1,2048]{1,0:T(1,128)S(1)} %bitcast.8, bf16[2048]{0:T(1024)(128)(2,1)S(1)} %copy-done.3, ...), custom_call_target="tpu_custom_call" | custom-call | tf_op jit(solution)/shard_map/pallas_call | solution.py:1068
  48.5 0.0 copy-done.7
  48.5 0.6 %multiply_convert_fusion = bf16[48,512]{1,0:T(8,128)(2,1)} fusion(f32[48,512]{1,0:T(8,128)S(1)} %shard_map.222, f32[512]{0:T(512)S(1)} %copy-done.7), kind=kLoop, calls=%fused_computation | loop fusion | flops 49152 | bytes 149504 | tf_op jit(solution)/shard_map/convert_element_type | solution.py:1165
Async XLA Ops:
  0.6 0.7 %copy-start.6 = (s32[48]{0:T(128)S(1)}, s32[48]{0:T(128)}, u32[]{:S(2)}) copy-start(s32[48]{0:T(128)} %param.24) | copy-start | bytes 580
  1.3 7.3 %copy-start = (bf16[256,64]{0,1:T(8,128)(2,1)S(1)}, bf16[256,64]{0,1:T(8,128)(2,1)}, u32[]{:S(2)}) copy-start(bf16[256,64]{0,1:T(8,128)(2,1)} %param.39) | copy-start | bytes 98308
  1.3 7.3 %copy-start.1 = (bf16[256,64]{0,1:T(8,128)(2,1)S(1)}, bf16[256,64]{0,1:T(8,128)(2,1)}, u32[]{:S(2)}) copy-start(bf16[256,64]{0,1:T(8,128)(2,1)} %param.40) | copy-start | bytes 98308
  1.3 7.3 %copy-start.2 = (f32[2048]{0:T(1024)S(1)}, f32[2048]{0:T(1024)}, u32[]{:S(2)}) copy-start(f32[2048]{0:T(1024)} %param.30) | copy-start | bytes 24580
  1.3 7.3 %copy-start.3 = (bf16[2048]{0:T(1024)(128)(2,1)S(1)}, bf16[2048]{0:T(1024)(128)(2,1)}, u32[]{:S(2)}) copy-start(bf16[2048]{0:T(1024)(128)(2,1)} %side_switch_in.1) | copy-start | bytes 12292
  1.3 7.3 %copy-start.4 = (s32[48,4]{0,1:T(4,128)S(1)}, s32[48,4]{0,1:T(4,128)}, u32[]{:S(2)}) copy-start(s32[48,4]{0,1:T(4,128)} %param.31) | copy-start | bytes 2308
  1.3 7.3 %copy-start.5 = (f32[48,4]{0,1:T(4,128)S(1)}, f32[48,4]{0,1:T(4,128)}, u32[]{:S(2)}) copy-start(f32[48,4]{0,1:T(4,128)} %param.32) | copy-start | bytes 2308
  8.7 39.8 %copy-start.7 = (f32[512]{0:T(512)S(1)}, f32[512]{0:T(512)}, u32[]{:S(2)}) copy-start(f32[512]{0:T(512)} %param.43) | copy-start | bytes 6148

commit v5 on v4

--- a/solution.py
+++ b/solution.py
@@ -402,6 +402,7 @@
     weights,
     state,
     columns,
+    query_columns,
     spread_even,
     spread_odd,
     values,
@@ -453,10 +454,14 @@
     query, key = project(0)
     value, gate = project(1)
     lanes = columns.shape[1]
-    for i, (x, scale) in enumerate([(query, 1.0), (key, width ** (-0.5))]):
-        turned = rotated(x, cosine, sine, width // 2) * scale
+
+    def flipped(x):
+        turned = rotated(x, cosine, sine, width // 2)
         padded = jnp.concatenate([turned, jnp.zeros((lanes - rows, total), jnp.float32)], 0)
-        columns[i * total : (i + 1) * total, :] = jnp.transpose(padded).astype(jnp.bfloat16)
+        return jnp.transpose(padded)
+
+    query_columns[...] = flipped(query)
+    columns[...] = (flipped(key) * width ** (-0.5)).astype(jnp.bfloat16)
     for head in range(heads):
         values[head] = value[:, head * width : (head + 1) * width]
 
@@ -465,13 +470,12 @@
     offset = jnp.where(target_lane >= lanes, 1, 0)
     buffers = [spread_even, spread_odd]
 
-    def widen(i, pair, half):
+    def widen(i, pair):
         pick = jnp.where(source_lane == offset + (i * chunk + 2 * pair), 1.0, 0.0)
-        span = slice(half * total, (half + 1) * total)
-        buffers[i % 2][pair, span] = dot(columns[span, :], pick.astype(jnp.bfloat16))
-
-    for pair in range(chunk):
-        widen(0, pair // 2, pair % 2)
+        buffers[i % 2][pair] = dot(columns[...], pick.astype(jnp.bfloat16))
+
+    for pair in range(chunk // 2):
+        widen(0, pair)
     for i in range(chunks):
         base = i * chunk
         piece = pl.ds(base, chunk)
@@ -479,16 +483,16 @@
             pltpu.make_async_copy(state_in.at[piece], state.at[piece], state_sem.at[i]).wait()
         wide = buffers[i % 2]
         for at in range(chunk):
-            if i + 1 < chunks:
-                widen(i + 1, at // 2, at % 2)
+            if i + 1 < chunks and at % 2 == 0:
+                widen(i + 1, at // 2)
             if at == chunk // 2:
                 part = pl.ds(base, chunk // 2)
                 fetch(state.at[part], state_out.at[part], out_sem)
             lane = (at % 2) * lanes
             for head in range(heads):
                 low, high = head * width, (head + 1) * width
-                q_cols = wide[at // 2, low:high, lane : lane + width]
-                k_cols = wide[at // 2, total + low : total + high, lane : lane + width]
+                q_cols = query_columns[low:high, base + at : base + at + 1]
+                k_cols = wide[at // 2, low:high, lane : lane + width]
                 v_row = values[head, base + at : base + at + 1, :]
                 new = decays[head] * state[base + at, head] + k_cols * v_row
                 state[base + at, head] = new
@@ -511,7 +515,7 @@
     rows, heads, width = state.shape[0], state.shape[1], state.shape[2]
     chunk, lanes = 8, 128
     cols = heads * width
-    wide = pltpu.VMEM((chunk // 2, 2 * cols, 2 * lanes), jnp.float32)
+    wide = pltpu.VMEM((chunk // 2, cols, 2 * lanes), jnp.float32)
     return pl.pallas_call(
         functools.partial(retain_body, chunk),
         out_shape=[
@@ -526,7 +530,8 @@
             pltpu.VMEM(lengths.shape, lengths.dtype),
             pltpu.VMEM((tokens.shape[1], 4 * cols), jnp.bfloat16),
             pltpu.VMEM(state.shape, state.dtype),
-            pltpu.VMEM((2 * cols, lanes), jnp.bfloat16),
+            pltpu.VMEM((cols, lanes), jnp.bfloat16),
+            pltpu.VMEM((cols, lanes), jnp.float32),
             wide,
             wide,
             pltpu.VMEM((heads, rows, width), jnp.float32),
@@ -594,6 +599,7 @@
 ):
     chips, tps, capacity, groups = dims
     steps = chips
+    downs = ((0, 1), (2,), (3,))
     rows, cols = own_tokens.shape
     model = cols * tps
     half = cols // 2
@@ -833,15 +839,18 @@
         for peer in plane:
             push(own, own, send_sem.at[HIDDEN], recv_sem.at[HIDDEN + group], peer)
 
-    def down_step(group):
+    def down_step(index):
+        members = [(step, at) for step in downs[index] for at in range(2)]
+        both = pl.ds(downs[index][0], len(downs[index]))
         with jax.named_scope("hidden_wait"):
-            arrived = hidden_all.at[pl.ds(0, tps - 1), group_steps(group)]
-            settle(arrived, recv_sem.at[HIDDEN + group])
-        if group == 0:
+            for step in downs[index]:
+                arrived = hidden_all.at[pl.ds(0, tps - 1), group_steps(step)]
+                settle(arrived, recv_sem.at[HIDDEN + step])
+        if index == 0:
             settle(down_w, weight_sem.at[4])
         spread_rows = []
         number = lax.broadcasted_iota(jnp.int32, (wide, pair_slots), 1).astype(jnp.float32)
-        for step in groups[group]:
+        for step in downs[index]:
             packed = jnp.concatenate([hidden_all[t, step] for t in range(tps)], 1)
             for at in range(2):
                 slot = column(group_at(step, at))
@@ -854,26 +863,25 @@
             mine = jnp.concatenate([r[e * rows : (e + 1) * rows] for r in spread_rows], 0)
             term = dot(mine, down_w[e])
             result = term if result is None else result + term
-        for i, (step, at) in enumerate(blocks(group)):
+        for i, (step, at) in enumerate(members):
             part = result[i * rows : (i + 1) * rows]
             if at == 0:
                 total[step] = part
             else:
                 pair_out[step] = part.astype(jnp.bfloat16)
-        both = group_steps(group)
         push(
             pair_out.at[both],
             pair_in.at[both],
             send_sem.at[9],
-            back_sem.at[group],
+            back_sem.at[index],
             partner,
         )
 
-    def return_step(group):
-        both = group_steps(group)
+    def return_step(index):
+        both = pl.ds(downs[index][0], len(downs[index]))
         with jax.named_scope("pair_wait"):
-            settle(pair_in.at[both], back_sem.at[group])
-        for step in groups[group]:
+            settle(pair_in.at[both], back_sem.at[index])
+        for step in downs[index]:
             mine = total[step] + pair_in[step].astype(jnp.float32)
             if step == 0:
                 total[step] = mine
@@ -964,6 +972,10 @@
         expert_step(1)
     with jax.named_scope("corner2"):
         corner(2)
+    with jax.named_scope("own_shared"):
+        own_shared()
+    with jax.named_scope("own_switch"):
+        switch = own_switch()
     with jax.named_scope("relay3"):
         relay(3)
     with jax.named_scope("arrive2"):
@@ -990,26 +1002,18 @@
         expert_step(3)
     with jax.named_scope("down_step0"):
         down_step(0)
+    with jax.named_scope("return_step0"):
+        return_step(0)
     with jax.named_scope("down_step1"):
         down_step(1)
-    with jax.named_scope("own_shared"):
-        own_shared()
-    with jax.named_scope("own_switch"):
-        switch = own_switch()
-    with jax.named_scope("return_step0"):
-        return_step(0)
+    with jax.named_scope("own_side"):
+        own_side()
+    with jax.named_scope("down_step2"):
+        down_step(2)
     with jax.named_scope("return_step1"):
         return_step(1)
-    with jax.named_scope("down_step2"):
-        down_step(2)
-    with jax.named_scope("own_side"):
-        own_side()
     with jax.named_scope("return_step2"):
         return_step(2)
-    with jax.named_scope("down_step3"):
-        down_step(3)
-    with jax.named_scope("return_step3"):
-        return_step(3)
     with jax.named_scope("own_extra"):
         extra = own_extra()
 

time: 49.3 us -> 47.9 us (0.972)
  Pallas kernels: 47.1 us -> 45.7 us
    pallas_call x1, Pallas kernels: 7.27 us -> 6.49 us  [retain_kernel(): pl.pallas_call(functools.partial(retain_body, chunk), out_shape=[jax.Shap...]
    pallas_call x1, Pallas kernels: 39.8 us -> 39.2 us  [mixer(): pl.pallas_call(functools.partial(mixer_body, (chips, tps, capacity, group...]
where the time goes in v5:
time: 47.9 us; the launch traced here: 47.7 us
  Pallas kernels  45.7 us (95%)
  between operations  0.74 us (2%)
  local copies, waits for them, and re-layouts  0.68 us (1%)
  other arithmetic  0.63 us (1%)
    pallas_call x1, Pallas kernels, mixer(): pl.pallas_call(functools.partial(mixer_body, (chips, tps, capacity, group...  39.2 us
    pallas_call x1, Pallas kernels, retain_kernel(): pl.pallas_call(functools.partial(retain_body, chunk), out_shape=[jax.Shap...  6.49 us

profile of v5, /device:TPU:0, one launch (start us, length us, event | category | flops | bytes accessed | tf_op | source)
XLA Modules:
  0.0 47.7 jit_solution(6780981788946580527)
XLA Ops:
  0.6 0.0 copy-start.6
  0.6 0.6 %copy-done.6 = s32[48]{0:T(128)S(1)} copy-done((s32[48]{0:T(128)S(1)}, s32[48]{0:T(128)}, u32[]{:S(2)}) %copy-start.6) | copy-done | bytes 216
  1.3 0.0 copy-start
  1.3 0.0 copy-start.1
  1.3 0.0 copy-start.2
  1.3 0.0 copy-start.3
  1.3 0.0 copy-start.4
  1.3 0.0 copy-start.5
  1.3 6.5 %shard_map.221 = (bf16[48,256]{1,0:T(8,128)(2,1)S(1)}, f32[48,4,64,64]{3,2,1,0:T(8,128)}) custom-call(bf16[48,2048]{1,0:T(8,128)(2,1)} %tokens_in.3, s32[1,48]{1,0:T(1,128)S(1)} %bitcast.11, bf16[2048,256]{1,0:T(8,128)(2,1)} %query_in.1, bf16[2048,256]{1,0:T(8,128)(2,1)} %key_in.1, bf16[2048,256]{1,0:T(8,128)(2,1)} %value_in.1, bf16[2048,256]{1,0:T(8,128)(2,1)} %gate_in.2, ...), custom_call_target="tpu_custom_call" | custom-call | tf_op jit(solution)/shard_map/pallas_call | solution.py:519
  7.8 0.0 copy-done
  7.8 0.0 copy-done.1
  7.8 0.0 copy-done.2
  7.8 0.0 copy-done.3
  7.9 0.0 copy-done.4
  7.9 0.0 copy-done.5
  7.9 0.0 copy-start.7
  7.9 39.2 %shard_map.222 = f32[48,512]{1,0:T(8,128)S(1)} custom-call(bf16[48,256]{1,0:T(8,128)(2,1)S(1)} %get-tuple-element.4.mixed_in, bf16[48,2048]{1,0:T(8,128)(2,1)} %tokens_in.3, s32[4,48]{1,0:T(4,128)S(1)} %bitcast.9, f32[4,48]{1,0:T(4,128)S(1)} %bitcast.10, f32[1,2048]{1,0:T(1,128)S(1)} %bitcast.8, bf16[2048]{0:T(1024)(128)(2,1)S(1)} %copy-done.3, ...), custom_call_target="tpu_custom_call" | custom-call | tf_op jit(solution)/shard_map/pallas_call | solution.py:1072
  47.1 0.0 copy-done.7
  47.1 0.6 %multiply_convert_fusion = bf16[48,512]{1,0:T(8,128)(2,1)} fusion(f32[48,512]{1,0:T(8,128)S(1)} %shard_map.222, f32[512]{0:T(512)S(1)} %copy-done.7), kind=kLoop, calls=%fused_computation | loop fusion | flops 49152 | bytes 149504 | tf_op jit(solution)/shard_map/convert_element_type | solution.py:1169
Async XLA Ops:
  0.6 0.7 %copy-start.6 = (s32[48]{0:T(128)S(1)}, s32[48]{0:T(128)}, u32[]{:S(2)}) copy-start(s32[48]{0:T(128)} %param.24) | copy-start | bytes 580
  1.3 6.5 %copy-start = (bf16[256,64]{0,1:T(8,128)(2,1)S(1)}, bf16[256,64]{0,1:T(8,128)(2,1)}, u32[]{:S(2)}) copy-start(bf16[256,64]{0,1:T(8,128)(2,1)} %param.39) | copy-start | bytes 98308
  1.3 6.5 %copy-start.1 = (bf16[256,64]{0,1:T(8,128)(2,1)S(1)}, bf16[256,64]{0,1:T(8,128)(2,1)}, u32[]{:S(2)}) copy-start(bf16[256,64]{0,1:T(8,128)(2,1)} %param.40) | copy-start | bytes 98308
  1.3 6.5 %copy-start.2 = (f32[2048]{0:T(1024)S(1)}, f32[2048]{0:T(1024)}, u32[]{:S(2)}) copy-start(f32[2048]{0:T(1024)} %param.30) | copy-start | bytes 24580
  1.3 6.6 %copy-start.3 = (bf16[2048]{0:T(1024)(128)(2,1)S(1)}, bf16[2048]{0:T(1024)(128)(2,1)}, u32[]{:S(2)}) copy-start(bf16[2048]{0:T(1024)(128)(2,1)} %side_switch_in.1) | copy-start | bytes 12292
  1.3 6.6 %copy-start.4 = (s32[48,4]{0,1:T(4,128)S(1)}, s32[48,4]{0,1:T(4,128)}, u32[]{:S(2)}) copy-start(s32[48,4]{0,1:T(4,128)} %param.31) | copy-start | bytes 2308
  1.3 6.6 %copy-start.5 = (f32[48,4]{0,1:T(4,128)S(1)}, f32[48,4]{0,1:T(4,128)}, u32[]{:S(2)}) copy-start(f32[48,4]{0,1:T(4,128)} %param.32) | copy-start | bytes 2308
  7.9 39.2 %copy-start.7 = (f32[512]{0:T(512)S(1)}, f32[512]{0:T(512)}, u32[]{:S(2)}) copy-start(f32[512]{0:T(512)} %param.43) | copy-start | bytes 6148
